TPU v7x, 32 devices: a whole 2x2x4 slice. The times are simulated.
32 devices in a mesh: fs: 4 (over z), rep: 4 (over y, x), tp: 2 (over core).
Axes of the slice: x: 2, y: 2, z: 4, core: 2. Of those that a mesh axis runs over, the one named last changes fastest.
Arguments:
- inputs: bfloat16 [4096, 2048], P(('fs', 'rep')), may hold values from -6 to 6
- cot_query: bfloat16 [4096, 2048], P(('fs', 'rep'), 'tp'), may hold values from -0.09375 to 0.09375
- cot_key: bfloat16 [4096, 512], P(('fs', 'rep'), 'tp'), may hold values from -0.09375 to 0.09375
- basis_query: bfloat16 [2048, 512], P('fs'), may hold values from -0.125 to 0.125
- basis_key: bfloat16 [2048, 512], P('fs'), may hold values from -0.125 to 0.125
- weight_query: float32 [2048, 2048], P('fs', 'tp'), may hold values from -0.125 to 0.125
- weight_key: float32 [2048, 512], P('fs', 'tp'), may hold values from -0.125 to 0.125
- moments_query: float32 [2, 512, 2048], P(None, 'fs', 'tp'), may hold values from -8 to 8, as said below
- moments_key: float32 [2, 512, 512], P(None, 'fs', 'tp'), may hold values from -8 to 8, as said below
Outputs:
- step_query: float32 [2048, 2048], P('fs', 'tp')
- step_key: float32 [2048, 512], P('fs', 'tp')
- new_weight_query: float32 [2048, 2048], P('fs', 'tp')
- new_weight_key: float32 [2048, 512], P('fs', 'tp')
- copy_query: bfloat16 [2048, 2048], P(None, 'tp')
- copy_key: bfloat16 [2048, 512], P(None, 'tp')
- new_moments_query: float32 [2, 512, 2048], P(None, 'fs', 'tp')
- new_moments_key: float32 [2, 512, 512], P(None, 'fs', 'tp')
Inputs may be any that keep to these rules, and one draw needn't show every extreme that they name: `moments_query`: entry 1 along the first dimension is positive. `moments_key`: entry 1 along the first dimension is positive.
All inputs are finite; a program needn't handle non-finite values.
Results may differ from a plain program's by a relative error of at most 0.009.
Values may be sent and summed in bfloat16 or wider, within the bound.
No kernel may reach another device: no remote copies, remote signals or barrier semaphores. Data moves between devices by JAX's collectives and lax.ppermute only.
A program may use at most 64 MiB of HBM per device.

v0:
```python
import jax
import jax.numpy as jnp
from jax import lax
from jax.sharding import PartitionSpec as P


def plain_contract(left, right):
    return lax.dot_general(
        left, right, (((0,), (0,)), ((), ())), preferred_element_type=jnp.float32
    )


def split_contract(values, cotangent):
    leading = values.astype(jnp.bfloat16)
    remainder = (values - leading.astype(jnp.float32)).astype(jnp.bfloat16)
    return plain_contract(leading, cotangent) + plain_contract(remainder, cotangent)


def moment_update(moments, grad_low):
    first = 0.9 * moments[0] + 0.1 * grad_low
    second = 0.95 * moments[1] + 0.05 * grad_low * grad_low
    normed = first / (jnp.sqrt(second) + 1e-08)
    return (jnp.stack([first, second]), normed)


def on_device(
    inputs,
    cot_query,
    cot_key,
    basis_query,
    basis_key,
    weight_query,
    weight_key,
    moments_query,
    moments_key,
):
    query_cols = cot_query.shape[1]
    whole_query, whole_key = (
        lax.all_gather(basis_query, "fs", axis=0, tiled=True),
        lax.all_gather(basis_key, "fs", axis=0, tiled=True),
    )
    token_query = jnp.dot(inputs, whole_query, preferred_element_type=jnp.float32)
    token_key = jnp.dot(inputs, whole_key, preferred_element_type=jnp.float32)
    low_terms = jnp.concatenate(
        [split_contract(token_query, cot_query), split_contract(token_key, cot_key)], axis=1
    )
    low = lax.psum_scatter(low_terms, "fs", scatter_dimension=0, tiled=True)
    low = lax.psum(low, "rep")
    new_moments_query, normed_query = moment_update(moments_query, low[:, :query_cols])
    new_moments_key, normed_key = moment_update(moments_key, low[:, query_cols:])
    totals = lax.psum(
        (jnp.sum(normed_query * normed_query), jnp.sum(normed_key * normed_key)), ("fs", "tp")
    )
    spread = lax.axis_size("fs") * lax.axis_size("tp")
    scale_query = lax.rsqrt(totals[0] / (normed_query.size * spread) + 1e-06)
    scale_key = lax.rsqrt(totals[1] / (normed_key.size * spread) + 1e-06)
    directions = jnp.concatenate(
        [normed_query.astype(jnp.bfloat16), normed_key.astype(jnp.bfloat16)], axis=1
    )
    piece = lax.all_gather(directions, "fs", axis=0, tiled=True)
    query_term = jnp.dot(basis_query, piece[:, :query_cols], preferred_element_type=jnp.float32)
    key_term = jnp.dot(basis_key, piece[:, query_cols:], preferred_element_type=jnp.float32)
    raw_step = jnp.concatenate([query_term, key_term], axis=1)
    step_query = scale_query * raw_step[:, :query_cols]
    step_key = scale_key * raw_step[:, query_cols:]
    new_weight_query = weight_query - 0.02 * step_query
    new_weight_key = weight_key - 0.02 * step_key
    copy_query, copy_key = (
        lax.all_gather(new_weight_query.astype(jnp.bfloat16), "fs", axis=0, tiled=True),
        lax.all_gather(new_weight_key.astype(jnp.bfloat16), "fs", axis=0, tiled=True),
    )
    return (
        step_query,
        step_key,
        new_weight_query,
        new_weight_key,
        copy_query,
        copy_key,
        new_moments_query,
        new_moments_key,
    )


def solution(mesh):
    in_specs = (
        P(("fs", "rep"), None),
        P(("fs", "rep"), "tp"),
        P(("fs", "rep"), "tp"),
        P("fs", None),
        P("fs", None),
        P("fs", "tp"),
        P("fs", "tp"),
        P(None, "fs", "tp"),
        P(None, "fs", "tp"),
    )
    out_specs = (
        P("fs", "tp"),
        P("fs", "tp"),
        P("fs", "tp"),
        P("fs", "tp"),
        P(None, "tp"),
        P(None, "tp"),
        P(None, "fs", "tp"),
        P(None, "fs", "tp"),
    )
    return jax.shard_map(
        on_device, mesh=mesh, in_specs=in_specs, out_specs=out_specs, check_vma=False
    )
```

profile of v0, /device:TPU:0, one launch (start us, length us, event | category | flops | bytes accessed | tf_op | source)
XLA Modules:
  0.0 373.1 jit_solution(2540141860126746444)
XLA Ops:
  7.2 0.7 all-gather.8.cloned.1.call-update
  8.0 0.7 all-gather.6.cloned.1.call-update
  8.7 49.3 %all-gather.8.cloned.1.call-done = bf16[2048,512]{1,0:T(8,128)(2,1)} async-done(((bf16[512,512]{1,0:T(8,128)(2,1)}), bf16[2048,512]{1,0:T(8,128)(2,1)}) %all-gather.8.cloned.1.call-update) | async-done | bytes 2097168 | tf_op jit(solution)/shard_map/all_gather | solution.py:40
  58.0 2.3 fusion.18
  60.3 0.3 fusion.6
  60.5 0.3 convolution_add_fusion.1
  60.8 43.2 %all-gather.6.cloned.1.call-done = bf16[2048,512]{1,0:T(8,128)(2,1)} async-done(((bf16[512,512]{1,0:T(8,128)(2,1)}), bf16[2048,512]{1,0:T(8,128)(2,1)}) %all-gather.6.cloned.1.call-update) | async-done | bytes 2097168 | tf_op jit(solution)/shard_map/all_gather | solution.py:39
  104.0 2.3 fusion.17
  106.3 0.5 fusion.9
  106.8 0.5 convolution_add_fusion
  107.3 1.7 pad_maximum_fusion
  109.0 51.2 %reduce-scatter.2.cloned.1.call-done = f32[128,1280]{1,0:T(8,128)} async-done(((f32[512,1280]{1,0:T(8,128)}), f32[128,1280]{1,0:T(8,128)}) %reduce-scatter.2.cloned.1.call-update) | async-done | bytes 655376 | tf_op jit(solution)/shard_map/reduce_scatter | solution.py:47
  160.3 49.2 %all-reduce.3.cloned.1.call-done = f32[128,1280]{1,0:T(8,128)} async-done(((f32[128,1280]{1,0:T(8,128)}), f32[128,1280]{1,0:T(8,128)}) %all-reduce.3.cloned.1.call-update) | async-done | bytes 655376 | tf_op jit(solution)/shard_map/psum | solution.py:48
  209.4 1.6 fusion.13
  211.1 2.9 fusion.11
  214.0 0.7 pad_maximum_fusion.2
  214.8 2.2 copy.20
  217.0 17.6 %all-reduce = (f32[]{:T(128)}, f32[]{:T(128)}) all-reduce(f32[]{:T(128)} %get-tuple-element.28, f32[]{:T(128)} %get-tuple-element.32), channel_id=1, replica_groups=mesh['fs'=4,'rep'=4,'tp'=2] {'fs','tp'}, use_global_device_ids=true, to_apply=%region_3.0 | all-reduce | flops 2 | bytes 16 | tf_op jit(solution)/shard_map/psum | solution.py:51
  235.2 12.4 %all-gather.10.cloned.1.call-done = bf16[512,1280]{1,0:T(8,128)(2,1)} async-done(((bf16[128,1280]{1,0:T(8,128)(2,1)}), bf16[512,1280]{1,0:T(8,128)(2,1)}) %all-gather.10.cloned.1.call-update) | async-done | bytes 1310736 | tf_op jit(solution)/shard_map/all_gather | solution.py:60
  247.6 2.7 fusion.15
  250.4 1.8 copy.19
  252.9 4.6 %fusion.16 = (bf16[512,1024]{0,1:T(8,128)(2,1)}, f32[512,1024]{0,1:T(8,128)S(1)}, f32[512,1024]{0,1:T(8,128)}) fusion(f32[512,1024]{0,1:T(8,128)} %copy.19, bf16[512,512]{1,0:T(8,128)(2,1)} %param.12, bf16[512,1280]{1,0:T(8,128)(2,1)} %all-gather.10.cloned.1.call-done, f32[]{:T(128)S(6)} %rsqrt.6), kind=kOutput, calls=%fused_computation.36 | convolution fusion | flops 538968064 | bytes 8912900 | tf_op jit(solution)/shard_map/dot_general | solution.py:61
  257.6 0.7 pad_maximum_fusion.3
  258.3 2.3 pad_maximum_fusion.1
  260.6 2.9 copy.21
  263.4 2.0 copy.22
  265.5 1.8 copy.23
  267.3 2.0 copy.24
  269.3 8.3 %all-gather.14.cloned.1.call-done = bf16[2048,256]{0,1:T(8,128)(2,1)} async-done(((bf16[512,256]{0,1:T(8,128)(2,1)}), bf16[2048,256]{0,1:T(8,128)(2,1)}) %all-gather.14.cloned.1.call-update) | async-done | bytes 1048592 | tf_op jit(solution)/shard_map/all_gather | solution.py:70
  277.6 2.3 copy.26
  279.8 80.0 %all-gather.12.cloned.1.call-done = bf16[2048,1024]{0,1:T(8,128)(2,1)} async-done(((bf16[512,1024]{0,1:T(8,128)(2,1)}), bf16[2048,1024]{0,1:T(8,128)(2,1)}) %all-gather.12.cloned.1.call-update) | async-done | bytes 4194320 | tf_op jit(solution)/shard_map/all_gather | solution.py:69
  359.9 6.4 %copy.25 = bf16[2048,1024]{1,0:T(8,128)(2,1)} copy(bf16[2048,1024]{0,1:T(8,128)(2,1)} %all-gather.12.cloned.1.call-done) | data formatting | bytes 8388608
  (24 shorter events, 0.4 us)
Async XLA Ops:
  7.2 50.8 %copy-start = (bf16[256,2048]{1,0:T(8,128)(2,1)S(1)}, bf16[256,2048]{1,0:T(8,128)(2,1)}, u32[]{:S(2)}) copy-start(bf16[256,2048]{1,0:T(8,128)(2,1)} %param.9) | copy-start | bytes 3145732
  7.2 50.8 %all-gather.8.cloned.1.call-start = ((), (), s32[]{:S(2)}) async-start(), calls=%async_computation.2 | async-start | bytes 2621440 | tf_op jit(solution)/shard_map/all_gather | solution.py:40
  7.9 52.4 %copy-start.4 = (bf16[256,256]{1,0:T(8,128)(2,1)S(1)}, bf16[256,256]{1,0:T(8,128)(2,1)}, u32[]{:S(2)}) copy-start(bf16[256,256]{1,0:T(8,128)(2,1)} %param.11) | copy-start | bytes 393220
  7.9 96.1 %all-gather.6.cloned.1.call-start = ((), (), s32[]{:S(2)}) async-start(), calls=%async_computation.1 | async-start | bytes 2621440 | tf_op jit(solution)/shard_map/all_gather | solution.py:39
  8.7 151.5 %reduce-scatter.2.cloned.1.call-start = ((), (), s32[]{:S(2)}) async-start(), calls=%async_computation.3 | async-start | bytes 3276800 | tf_op jit(solution)/shard_map/reduce_scatter | solution.py:47
  60.8 45.5 %copy-start.2 = (bf16[256,1024]{1,0:T(8,128)(2,1)S(1)}, bf16[256,1024]{1,0:T(8,128)(2,1)}, u32[]{:S(2)}) copy-start(bf16[256,1024]{1,0:T(8,128)(2,1)} %param.10) | copy-start | bytes 1572868
  109.0 100.5 %copy-start.5 = (f32[2,128,256]{2,1,0:T(8,128)S(1)}, f32[2,128,256]{2,1,0:T(8,128)}, u32[]{:S(2)}) copy-start(f32[2,128,256]{2,1,0:T(8,128)} %param.17) | copy-start | bytes 786436
  109.0 102.1 %copy-start.3 = (f32[2,128,1024]{2,1,0:T(8,128)S(1)}, f32[2,128,1024]{2,1,0:T(8,128)}, u32[]{:S(2)}) copy-start(f32[2,128,1024]{2,1,0:T(8,128)} %param.16) | copy-start | bytes 3145732
  109.0 100.4 %all-reduce.3.cloned.1.call-start = ((), (), s32[]{:S(2)}) async-start(), calls=%async_computation.4 | async-start | bytes 1310720 | tf_op jit(solution)/shard_map/psum | solution.py:48
  160.2 87.4 %all-gather.10.cloned.1.call-start = ((), (), s32[]{:S(2)}) async-start(), calls=%async_computation.5 | async-start | bytes 1638400 | tf_op jit(solution)/shard_map/all_gather | solution.py:60
  214.7 35.7 %copy-start.1 = (f32[512,1024]{1,0:T(8,128)S(1)}, f32[512,1024]{1,0:T(8,128)}, u32[]{:S(2)}) copy-start(f32[512,1024]{1,0:T(8,128)} %param.14) | copy-start | bytes 6291460
  214.8 62.8 %all-gather.14.cloned.1.call-start = ((), (), s32[]{:S(2)}) async-start(), calls=%async_computation.7 | async-start | bytes 1310720 | tf_op jit(solution)/shard_map/all_gather | solution.py:70
  250.4 109.5 %all-gather.12.cloned.1.call-start = ((), (), s32[]{:S(2)}) async-start(), calls=%async_computation.6 | async-start | bytes 5242880 | tf_op jit(solution)/shard_map/all_gather | solution.py:69
Sparse Core Ops, SparseCore 0:
  9.6 48.3 all-gather.7
  59.5 44.4 all-gather.5
  109.1 51.0 reduce-scatter.1
  163.1 46.3 all-reduce.2
  214.9 32.7 all-gather.9
  250.5 27.0 all-gather.13
  279.7 80.1 all-gather.11
where the time goes:
time: 374 us; the launch traced here: 373 us
  waiting for transfers between devices  295 us (79%)
  local copies, waits for them, and re-layouts  21.4 us (6%)
  blocking collectives  17.6 us (5%)
  between operations  15.6 us (4%)
  matrix products  13.3 us (4%)
  other arithmetic  9.97 us (3%)
    all_gather x1, waiting for transfers between devices, on_device(): lax.all_gather(new_weight_query.astype(jnp.bfloat16), 'fs', axis=0, tiled...  80 us
    reduce_scatter x1, waiting for transfers between devices, on_device(): low = lax.psum_scatter(low_terms, 'fs', scatter_dimension=0, tiled=True)  51.2 us
    all_gather x1, waiting for transfers between devices, on_device(): lax.all_gather(basis_key, 'fs', axis=0, tiled=True)  49.3 us
    psum x1, waiting for transfers between devices, on_device(): low = lax.psum(low, 'rep')  49.2 us
    all_gather x1, waiting for transfers between devices, on_device(): lax.all_gather(basis_query, 'fs', axis=0, tiled=True)  43.2 us
    unnamed x20, local copies, waits for them, and re-layouts  21.4 us
    psum x1, blocking collectives, on_device(): lax.psum((jnp.sum(normed_query * normed_query), jnp.sum(normed_key * norm...  17.6 us
    all_gather x1, waiting for transfers between devices, on_device(): piece = lax.all_gather(directions, 'fs', axis=0, tiled=True)  12.4 us
  transfers between devices with their start and end apart: 7, of which 7 were waited for; matrix products, arithmetic and copies ran while one was open for 7% of the time, Pallas kernels for 0%

commit v1 on v0

v1 whole, which is shorter than its diff:
```python
import functools

import jax
import jax.numpy as jnp
from jax import lax
from jax.experimental import pallas as pl
from jax.experimental.pallas import tpu as pltpu
from jax.sharding import PartitionSpec as P


BF = jnp.bfloat16
F32 = jnp.float32
SMALL = pltpu.CompilerParams(vmem_limit_bytes=16 * 2**20)
LARGE = pltpu.CompilerParams(vmem_limit_bytes=30 * 2**20)


def whole(a):
    shape = getattr(a, "shape", a)
    return pl.BlockSpec(tuple(shape), lambda *_: (0,) * len(shape))


def contract(left, right):
    return lax.dot_general(left, right, (((0,), (0,)), ((), ())), preferred_element_type=F32)


def xor_swap(value, axis, bit):
    size = lax.axis_size(axis)
    return lax.ppermute(value, axis, [(i, i ^ bit) for i in range(size)])


def exchange(value, axis):
    return lax.all_to_all(value, axis, 0, 0, tiled=True)


def spread(own):
    own = own[None]
    rest, rels = None, []
    bit = lax.axis_size("fs") // 2
    while bit:
        near = xor_swap(own, "fs", bit)
        if rest is None:
            rest, rels = near, [bit]
        elif bit > 1:
            far = xor_swap(rest, "fs", bit)
            rest = jnp.concatenate([rest, near, far], axis=0)
            rels = rels + [bit] + [i ^ bit for i in rels]
        else:
            far = xor_swap(rest, "fs", bit)
            return [([bit], near), (rels, rest), ([i ^ bit for i in rels], far)]
        bit //= 2
    return [(rels, rest)]


def parity(r):
    return jnp.bitwise_xor(jnp.bitwise_and(r, 1), jnp.right_shift(r, 1))


def share(r):
    return (2 * parity(r), 2) if lax.axis_size("rep") == 4 else (r, 1)


def spread_planes(own):
    n_r = lax.axis_size("rep")
    pieces = []
    for rels, got in spread(own):
        pieces.append((rels, got, lambda r: share(r)[0]))
        if n_r == 4:
            h = got.shape[1] // 2
            near = xor_swap(got[:, :h], "rep", 1)
            pieces.append((rels, near, lambda r: 2 - 2 * parity(r)))
            near = xor_swap(got[:, h:], "rep", 2)
            pieces.append((rels, near, lambda r: 3 - 2 * parity(r)))
        else:
            for i in range(1, n_r):
                near = xor_swap(got, "rep", i)
                pieces.append((rels, near, lambda r, i=i: jnp.bitwise_xor(r, i)))
    return pieces


def token_kernel(rels, z_ref, r_ref, x_ref, own_ref, *refs):
    parts, (basis_ref, token_ref), (x_vmem, sem) = refs[:-4], refs[-4:-2], refs[-2:]
    load = pltpu.make_async_copy(x_ref, x_vmem, sem)
    load.start()
    z = z_ref[0]
    rows = own_ref.shape[0]
    basis_ref[pl.ds(pl.multiple_of(z * rows, rows), rows), :] = own_ref[...]
    for (rel, first), part in zip(rels, parts):
        size = part.shape[1]
        for j, rel_j in enumerate(rel):
            at = jnp.bitwise_xor(z, rel_j) * rows + first(r_ref[0]) * (rows // lax.axis_size("rep"))
            basis_ref[pl.ds(pl.multiple_of(at, 16), size), :] = part[j]
    load.wait()
    token_ref[...] = jnp.dot(x_vmem[...], basis_ref[...], preferred_element_type=F32).astype(BF)


def tokens(z, r, x, own, parts):
    return pl.pallas_call(
        functools.partial(token_kernel, tuple((tuple(rel), first) for rel, _, first in parts)),
        in_specs=[pl.BlockSpec(memory_space=pltpu.SMEM)] * 2
        + [pl.BlockSpec(memory_space=pltpu.HBM), whole(own)]
        + [whole(p) for _, p, _ in parts],
        out_specs=[whole((x.shape[1], own.shape[1])), whole((x.shape[0], own.shape[1]))],
        grid=(1,),
        out_shape=[
            jax.ShapeDtypeStruct((x.shape[1], own.shape[1]), BF),
            jax.ShapeDtypeStruct((x.shape[0], own.shape[1]), BF),
        ],
        scratch_shapes=[pltpu.VMEM(x.shape, BF), pltpu.SemaphoreType.DMA],
        compiler_params=SMALL,
        name="tokens",
    )(z, r, x, own, *[p for _, p, _ in parts])


def terms_kernel(t_ref, mine_ref, other_ref, cq_ref, ck_ref, out_ref):
    n_r, n_f, rows, _ = out_ref.shape
    cols_q = cq_ref.shape[1]
    query_mine = t_ref[0] == 0
    mine, other = mine_ref[...], other_ref[...]
    q = contract(jnp.where(query_mine, mine, other), cq_ref[...]).astype(BF)
    k = contract(jnp.where(query_mine, other, mine), ck_ref[...]).astype(BF)
    for j in range(n_f):
        for i in range(n_r):
            at = (j * n_r + i) * rows
            out_ref[i, j, :, :cols_q] = q[at : at + rows]
            out_ref[i, j, :, cols_q:] = k[at : at + rows]


def terms(t, mine, other, cot_q, cot_k):
    n_f, n_r = lax.axis_size("fs"), lax.axis_size("rep")
    shape = (n_r, n_f, mine.shape[1] // (n_f * n_r), cot_q.shape[1] + cot_k.shape[1])
    return pl.pallas_call(
        terms_kernel,
        in_specs=[pl.BlockSpec(memory_space=pltpu.SMEM)]
        + [whole(a) for a in (mine, other, cot_q, cot_k)],
        out_specs=whole(shape),
        grid=(1,),
        out_shape=jax.ShapeDtypeStruct(shape, BF),
        compiler_params=SMALL,
        name="terms",
    )(t, mine, other, cot_q, cot_k)


def sum_kernel(in_ref, out_ref):
    total = in_ref[0].astype(F32)
    for i in range(1, in_ref.shape[0]):
        total = total + in_ref[i].astype(F32)
    out_ref[...] = total.astype(BF)


def sum_first(value):
    return pl.pallas_call(
        sum_kernel,
        in_specs=[whole(value)],
        out_specs=whole(value.shape[1:]),
        grid=(1,),
        out_shape=jax.ShapeDtypeStruct(value.shape[1:], BF),
        compiler_params=SMALL,
        name="sum_first",
    )(value)


def moment_update(first, second, low):
    first = 0.9 * first + 0.1 * low
    second = 0.95 * second + 0.05 * low * low
    return first, second, first / (jnp.sqrt(second) + 1e-08)


def piece_kernel(got_ref, mq_ref, mk_ref, low_ref, out_ref):
    cols_q = mq_ref.shape[2]
    total = got_ref[0].astype(F32)
    for i in range(1, got_ref.shape[0]):
        total = total + got_ref[i].astype(F32)
    low = total.astype(BF)
    low_ref[...] = low
    low = low.astype(F32)
    q = moment_update(mq_ref[0], mq_ref[1], low[:, :cols_q])[2].astype(BF)
    k = moment_update(mk_ref[0], mk_ref[1], low[:, cols_q:])[2].astype(BF)
    for i in range(out_ref.shape[0]):
        out_ref[i, :, :cols_q] = q
        out_ref[i, :, cols_q:] = k


def piece(r, got, moments_q, moments_k):
    n_f, rows, cols = got.shape
    moments_q = lax.dynamic_slice_in_dim(moments_q, r * rows, rows, 1)
    moments_k = lax.dynamic_slice_in_dim(moments_k, r * rows, rows, 1)
    return pl.pallas_call(
        piece_kernel,
        in_specs=[whole(got), whole(moments_q), whole(moments_k)],
        out_specs=[whole((rows, cols)), whole((n_f, rows, cols))],
        grid=(1,),
        out_shape=[
            jax.ShapeDtypeStruct((rows, cols), BF),
            jax.ShapeDtypeStruct((n_f, rows, cols), BF),
        ],
        compiler_params=SMALL,
        name="piece",
    )(got, moments_q, moments_k)


def plane_kernel(z_ref, got_ref, low_ref, out_ref):
    for i in range(out_ref.shape[0]):
        out_ref[i] = got_ref[...]
        out_ref[i, z_ref[0]] = low_ref[...]


def plane(z, got, low):
    return pl.pallas_call(
        plane_kernel,
        in_specs=[pl.BlockSpec(memory_space=pltpu.SMEM), whole(got), whole(low)],
        out_specs=whole((lax.axis_size("rep"), *got.shape)),
        grid=(1,),
        out_shape=jax.ShapeDtypeStruct((lax.axis_size("rep"), *got.shape), BF),
        compiler_params=SMALL,
        name="plane",
    )(z, got, low)


def squares(value):
    rows, cols = value.shape
    total = jnp.sum(jnp.square(value).reshape(rows // 8, 8, cols), axis=0)
    parts = [total[:, i : i + 128] for i in range(0, cols, 128)]
    return functools.reduce(jnp.add, parts)


def directions_kernel(z_ref, got_ref, mq_ref, mk_ref, nq_ref, nk_ref, dq_ref, dk_ref, sums_ref):
    n_r, n_f, rows, _ = got_ref.shape
    cols_q = mq_ref.shape[2]
    z = z_ref[0]
    own = n_r * rows
    for j in range(n_f):
        got = jnp.concatenate([got_ref[i, j] for i in range(n_r)], axis=0)
        dq_ref[j * own : (j + 1) * own, :] = got[:, :cols_q]
        dk_ref[j * own : (j + 1) * own, :] = got[:, cols_q:]
    low = jnp.concatenate([got_ref[i, z] for i in range(n_r)], axis=0).astype(F32)
    q = moment_update(mq_ref[0], mq_ref[1], low[:, :cols_q])
    k = moment_update(mk_ref[0], mk_ref[1], low[:, cols_q:])
    nq_ref[0], nq_ref[1] = q[0], q[1]
    nk_ref[0], nk_ref[1] = k[0], k[1]
    at = pl.ds(pl.multiple_of(z * own, own), own)
    dq_ref[at, :] = q[2].astype(BF)
    dk_ref[at, :] = k[2].astype(BF)
    sums_ref[:8, :] = squares(dq_ref[...].astype(F32))
    sums_ref[8:, :] = squares(dk_ref[...].astype(F32))


def directions(z, got, moments_q, moments_k):
    n_r, n_f, rows, _ = got.shape
    rank = n_r * n_f * rows
    return pl.pallas_call(
        directions_kernel,
        in_specs=[pl.BlockSpec(memory_space=pltpu.SMEM), whole(got), whole(moments_q), whole(moments_k)],
        out_specs=[
            whole(moments_q),
            whole(moments_k),
            whole((rank, moments_q.shape[2])),
            whole((rank, moments_k.shape[2])),
            whole((16, 128)),
        ],
        grid=(1,),
        out_shape=[
            jax.ShapeDtypeStruct(moments_q.shape, F32),
            jax.ShapeDtypeStruct(moments_k.shape, F32),
            jax.ShapeDtypeStruct((rank, moments_q.shape[2]), BF),
            jax.ShapeDtypeStruct((rank, moments_k.shape[2]), BF),
            jax.ShapeDtypeStruct((16, 128), F32),
        ],
        compiler_params=SMALL,
        name="directions",
    )(z, got, moments_q, moments_k)


def finish_kernel(
    plan, n_f, n_tp, z_ref, r_ref, t_ref, sums_ref, other_sums_ref, dq_ref, dk_ref,
    mine_ref, other_ref, wq_ref, wk_ref, *refs,
):
    n = len(plan)
    pieces, outs = refs[:n], refs[n : n + 6]
    basis, weights, held = refs[n + 6 : n + 8], refs[n + 8 : n + 10], refs[n + 10 : 2 * n + 10]
    results, copies_out = refs[2 * n + 10 : 2 * n + 14], refs[2 * n + 14 : 2 * n + 16]
    basis_sem, weight_sem, held_sem, out_sem, copy_sem = refs[2 * n + 16 :]
    z, r = z_ref[0], r_ref[0]
    rows, cols_q = wq_ref.shape
    cols_k = wk_ref.shape[1]
    rank = dq_ref.shape[0]
    h = rows // lax.axis_size("rep")
    order = [rel for rel in range(1, n_f)]
    order = [*order[:1], 0, *order[1:]]

    def block(rel):
        return pl.ds(pl.multiple_of(jnp.bitwise_xor(z, rel) * rows, rows), rows)

    def basis_load(rel, step):
        at = block(rel)
        for mat in range(2):
            for first, source in ((0, mine_ref), (1, other_ref)):

                @pl.when((t_ref[0] == 0) == (mat == first))
                def _():
                    pltpu.make_async_copy(
                        source.at[at], basis[mat].at[step], basis_sem.at[mat, step]
                    ).start()

    weight_loads = [
        pltpu.make_async_copy(source, to, weight_sem.at[i])
        for i, (source, to) in enumerate(zip((wq_ref, wk_ref), weights))
    ]
    held_loads = {}
    for i, (rels, _) in enumerate(plan):
        for j, rel in enumerate(rels):
            held_loads[i, rel] = pltpu.make_async_copy(
                pieces[i].at[j], held[i].at[j], held_sem.at[i, j]
            )
    for step, rel in enumerate(order):
        basis_load(rel, step)
        if rel == 0:
            for load in weight_loads:
                load.start()
        for i, (rels, _) in enumerate(plan):
            if rel in rels:
                held_loads[i, rel].start()

    def scale(at, cols):
        total = jnp.sum(sums_ref[at, :] + other_sums_ref[at, :], keepdims=True)
        return lax.rsqrt(total / (rank * cols * n_tp) + 1e-06)

    scales = scale(slice(0, 8), cols_q), scale(slice(8, 16), cols_k)
    directions = dq_ref, dk_ref
    stores = []
    for step, rel in enumerate(order):
        for mat in range(2):
            pltpu.make_async_copy(
                mine_ref.at[pl.ds(0, rows)], basis[mat].at[step], basis_sem.at[mat, step]
            ).wait()
        if rel == 0:
            for mat in range(2):
                product = jnp.dot(
                    basis[mat][step], directions[mat][...], preferred_element_type=F32
                )
                product = scales[mat] * product
                results[mat][...] = product
                weight_loads[mat].wait()
                new = weights[mat][...] - 0.02 * product
                results[2 + mat][...] = new
                copies_out[mat][step] = new.astype(BF)
                for i in (mat, 2 + mat):
                    store = pltpu.make_async_copy(results[i], outs[i], out_sem.at[i])
                    store.start()
                    stores.append(store)
        else:
            for i, (rels, first) in enumerate(plan):
                if rel not in rels:
                    continue
                held_loads[i, rel].wait()
                j = rels.index(rel)
                size = held[i].shape[1]
                at = pl.ds(pl.multiple_of(first(r) * h, 16), size)
                for mat in range(2):
                    part = slice(0, cols_q) if mat == 0 else slice(cols_q, cols_q + cols_k)
                    product = jnp.dot(
                        basis[mat][step, at, :], directions[mat][...], preferred_element_type=F32
                    )
                    new = held[i][j, :, part].astype(F32) - (0.02 * scales[mat]) * product
                    copies_out[mat][step, at, :] = new.astype(BF)
        for mat in range(2):
            store = pltpu.make_async_copy(
                copies_out[mat].at[step], outs[4 + mat].at[block(rel)], copy_sem.at[mat, step]
            )
            store.start()
            stores.append(store)
    for store in stores:
        store.wait()


def finish(z, r, t, sums, other_sums, dir_q, dir_k, mine, other, weight_q, weight_k, pieces):
    n_f, n_tp = lax.axis_size("fs"), lax.axis_size("tp")
    rows, cols_q = weight_q.shape
    cols_k = weight_k.shape[1]
    rank = mine.shape[1]
    plan = tuple((tuple(rels), first) for rels, _, first in pieces)
    arrays = [a for _, a, _ in pieces]
    hbm = pl.BlockSpec(memory_space=pltpu.HBM)
    smem = pl.BlockSpec(memory_space=pltpu.SMEM)
    shapes = [
        ((rows, cols_q), F32),
        ((rows, cols_k), F32),
        ((rows, cols_q), F32),
        ((rows, cols_k), F32),
        ((rows * n_f, cols_q), BF),
        ((rows * n_f, cols_k), BF),
    ]
    count = max(len(rels) for rels, _ in plan)
    return pl.pallas_call(
        functools.partial(finish_kernel, plan, n_f, n_tp),
        grid=(1,),
        in_specs=[smem] * 3
        + [whole(a) for a in (sums, other_sums, dir_q, dir_k)]
        + [hbm] * (4 + len(arrays)),
        out_specs=[hbm] * 6,
        out_shape=[jax.ShapeDtypeStruct(*s) for s in shapes],
        scratch_shapes=[
            *[pltpu.VMEM((n_f, rows, rank), BF)] * 2,
            pltpu.VMEM((rows, cols_q), F32),
            pltpu.VMEM((rows, cols_k), F32),
            *[pltpu.VMEM(a.shape, BF) for a in arrays],
            *[pltpu.VMEM(*s) for s in shapes[:4]],
            pltpu.VMEM((n_f, rows, cols_q), BF),
            pltpu.VMEM((n_f, rows, cols_k), BF),
            pltpu.SemaphoreType.DMA((2, n_f)),
            pltpu.SemaphoreType.DMA((2,)),
            pltpu.SemaphoreType.DMA((len(arrays), count)),
            pltpu.SemaphoreType.DMA((4,)),
            pltpu.SemaphoreType.DMA((2, n_f)),
        ],
        compiler_params=LARGE,
        name="finish",
    )(z, r, t, sums, other_sums, dir_q, dir_k, mine, other, weight_q, weight_k, *arrays)


def on_device(
    inputs,
    cot_query,
    cot_key,
    basis_query,
    basis_key,
    weight_query,
    weight_key,
    moments_query,
    moments_key,
):
    n_r = lax.axis_size("rep")
    z, r, t = lax.axis_index("fs"), lax.axis_index("rep"), lax.axis_index("tp")
    own_rows, _ = basis_query.shape
    h = own_rows // n_r
    at_z, at_r, at_t = (i.astype(jnp.int32)[None] for i in (z, r, t))
    first, count = share(r)

    own = jnp.where(t == 0, basis_query, basis_key)
    parts = spread_planes(lax.dynamic_slice_in_dim(own, first * h, count * h, 0))

    mine = [
        lax.dynamic_slice_in_dim(w, first * h, count * h, 0).astype(BF)
        for w in (weight_query, weight_key)
    ]
    pieces = spread_planes(jnp.concatenate(mine, axis=1))

    basis, token = tokens(at_z, at_r, inputs, own, parts)
    other_token = xor_swap(token, "tp", 1)
    other_basis = xor_swap(basis, "tp", 1)
    low = exchange(terms(at_t, token, other_token, cot_query, cot_key), "rep")
    low = exchange(sum_first(low), "fs")
    low, rows = piece(r, low, moments_query, moments_key)
    rows = plane(at_z, exchange(rows, "fs"), low)
    rows = exchange(rows, "rep")
    new_q, new_k, dir_q, dir_k, sums = directions(at_z, rows, moments_query, moments_key)
    other_sums = xor_swap(sums, "tp", 1)
    outs = finish(
        at_z, at_r, at_t, sums, other_sums, dir_q, dir_k, basis, other_basis,
        weight_query, weight_key, pieces,
    )
    return (*outs, new_q, new_k)


def solution(mesh):
    in_specs = (
        P(("fs", "rep"), None),
        P(("fs", "rep"), "tp"),
        P(("fs", "rep"), "tp"),
        P("fs", None),
        P("fs", None),
        P("fs", "tp"),
        P("fs", "tp"),
        P(None, "fs", "tp"),
        P(None, "fs", "tp"),
    )
    out_specs = (
        P("fs", "tp"),
        P("fs", "tp"),
        P("fs", "tp"),
        P("fs", "tp"),
        P(None, "tp"),
        P(None, "tp"),
        P(None, "fs", "tp"),
        P(None, "fs", "tp"),
    )

    return jax.shard_map(
        on_device, mesh=mesh, in_specs=in_specs, out_specs=out_specs, check_vma=False
    )
```

time: 374 us -> 147 us (0.39)
  waiting for transfers between devices: 295 us -> 65.2 us
  starting transfers between devices: 0.28 us -> 47.3 us
  blocking collectives: 17.6 us -> 0 us
  Pallas kernels: 0 us -> 15.7 us
  between operations: 15.6 us -> 0.78 us
  matrix products: 13.3 us -> 0 us
  other arithmetic: 9.97 us -> 2.07 us
  local copies, waits for them, and re-layouts: 21.4 us -> 15.1 us
    all_gather x5 -> x0, waiting for transfers between devices: 193 us -> none  [the longest x1 80 us: on_device(): lax.all_gather(new_weight_query.astype(jnp.bfloat16), 'fs', axis=0, tiled...]
    reduce_scatter x1 -> x0, waiting for transfers between devices: 51.2 us -> none  [on_device(): low = lax.psum_scatter(low_terms, 'fs', scatter_dimension=0, tiled=True)]
    psum x1 -> x0, waiting for transfers between devices: 49.2 us -> none  [on_device(): low = lax.psum(low, 'rep')]
    all_to_all x0 -> x4, waiting for transfers between devices: none -> 33.8 us  [exchange(): return lax.all_to_all(value, axis, 0, 0, tiled=True)]
    ppermute x0 -> x21, waiting for transfers between devices: none -> 31.4 us  [xor_swap(): return lax.ppermute(value, axis, [(i, i ^ bit) for i in range(size)])]
    ppermute x0 -> x21, starting transfers between devices: none -> 29.4 us  [xor_swap(): return lax.ppermute(value, axis, [(i, i ^ bit) for i in range(size)])]
    all_to_all x0 -> x4, starting transfers between devices: none -> 17.9 us  [exchange(): return lax.all_to_all(value, axis, 0, 0, tiled=True)]
    psum x1 -> x0, blocking collectives: 17.6 us -> none  [on_device(): lax.psum((jnp.sum(normed_query * normed_query), jnp.sum(normed_key * norm...]
  transfers between devices with their start and end apart: 7 -> 25, of which waited for: 7 -> 15; matrix products, arithmetic and copies ran while one was open for 7% -> 8% of each run, Pallas kernels for 0% -> 3%
where the time goes in v1:
time: 147 us; the launch traced here: 146 us
  waiting for transfers between devices  65.2 us (44%)
  starting transfers between devices  47.3 us (32%)
  Pallas kernels  15.7 us (11%)
  local copies, waits for them, and re-layouts  15.1 us (10%)
  other arithmetic  2.07 us (1%)
    all_to_all x4, waiting for transfers between devices, exchange(): return lax.all_to_all(value, axis, 0, 0, tiled=True)  33.8 us
    ppermute x21, waiting for transfers between devices, xor_swap(): return lax.ppermute(value, axis, [(i, i ^ bit) for i in range(size)])  31.4 us
    ppermute x21, starting transfers between devices, xor_swap(): return lax.ppermute(value, axis, [(i, i ^ bit) for i in range(size)])  29.4 us
    all_to_all x4, starting transfers between devices, exchange(): return lax.all_to_all(value, axis, 0, 0, tiled=True)  17.9 us
    pallas_call x1, Pallas kernels, finish(): pl.pallas_call(functools.partial(finish_kernel, plan, n_f, n_tp), grid=(1...  8.42 us
    slice x6, local copies, waits for them, and re-layouts, spread_planes(): near = xor_swap(got[:, h:], 'rep', 2)  7.95 us
    unnamed x20, local copies, waits for them, and re-layouts  4.23 us
  transfers between devices with their start and end apart: 25, of which 15 were waited for; matrix products, arithmetic and copies ran while one was open for 8% of the time, Pallas kernels for 3%

profile of v1, /device:TPU:0, one launch (start us, length us, event | category | flops | bytes accessed | tf_op | source)
XLA Modules:
  0.0 146.1 jit_solution(5689964881230017125)
XLA Ops:
  1.9 4.1 %collective-permute-start.3 = (bf16[1,256,512]{2,1,0:T(8,128)(2,1)S(1)}, bf16[1,256,512]{2,1,0:T(8,128)(2,1)S(1)}, u32[]{:S(2)}, u32[]{:S(2)}) collective-permute-start(bf16[1,256,512]{2,1,0:T(8,128)(2,1)S(1)} %dynamic-slice_bitcast_fusion), channel_id=1, source_target_pairs={{0,16},{8,24},{16,0},{24,8},{1,17},{9,25},{17,1},{25,9},{2,18},{10... | collective-permute-start | bytes 786440 | tf_op jit(solution)/shard_map/ppermute | solution.py:28
  6.0 1.6 %collective-permute-start = (bf16[1,256,512]{2,1,0:T(8,128)(2,1)S(1)}, bf16[1,256,512]{2,1,0:T(8,128)(2,1)S(1)}, u32[]{:S(2)}, u32[]{:S(2)}) collective-permute-start(bf16[1,256,512]{2,1,0:T(8,128)(2,1)S(1)} %dynamic-slice_bitcast_fusion), channel_id=1, source_target_pairs={{0,8},{8,0},{16,24},{24,16},{1,9},{9,1},{17,25},{25,17},{2,10},{10... | collective-permute-start | bytes 786440 | tf_op jit(solution)/shard_map/ppermute | solution.py:28
  7.6 10.4 %collective-permute-done.3.refs_3_ = bf16[1,256,512]{2,1,0:T(8,128)(2,1)S(1)} collective-permute-done((bf16[1,256,512]{2,1,0:T(8,128)(2,1)S(1)}, bf16[1,256,512]{2,1,0:T(8,128)(2,1)S(1)}, u32[]{:S(2)}, u32[]{:S(2)}) %collective-permute-start.3) | collective-permute-done | bytes 262176 | tf_op jit(solution)/shard_map/ppermute | solution.py:28
  19.3 1.5 %collective-permute-start.5 = (bf16[1,128,512]{2,1,0:T(8,128)(2,1)S(1)}, bf16[1,128,512]{2,1,0:T(8,128)(2,1)S(1)}, u32[]{:S(2)}, u32[]{:S(2)}) collective-permute-start(bf16[1,128,512]{2,1,0:T(8,128)(2,1)S(1)} %get-tuple-element.46), channel_id=1, source_target_pairs={{0,4},{2,6},{4,0},{6,2},{1,5},{3,7},{5,1},{7,3},{8,12},{10,14},{12... | collective-permute-start | bytes 393224 | tf_op jit(solution)/shard_map/ppermute | solution.py:28
  20.9 1.5 %collective-permute-start.4 = (bf16[1,128,512]{2,1,0:T(8,128)(2,1)}, bf16[1,128,512]{2,1,0:T(8,128)(2,1)S(1)}, u32[]{:S(2)}, u32[]{:S(2)}) collective-permute-start(bf16[1,128,512]{2,1,0:T(8,128)(2,1)} %get-tuple-element.47), channel_id=1, source_target_pairs={{0,2},{2,0},{4,6},{6,4},{1,3},{3,1},{5,7},{7,5},{8,10},{10,8},{12,... | collective-permute-start | bytes 393224 | tf_op jit(solution)/shard_map/ppermute | solution.py:28
  27.5 1.5 %collective-permute-start.7 = (bf16[1,128,512]{2,1,0:T(8,128)(2,1)}, bf16[1,128,512]{2,1,0:T(8,128)(2,1)}, u32[]{:S(2)}, u32[]{:S(2)}) collective-permute-start(bf16[1,128,512]{2,1,0:T(8,128)(2,1)} %get-tuple-element.45), channel_id=1, source_target_pairs={{0,2},{2,0},{4,6},{6,4},{1,3},{3,1},{5,7},{7,5},{8,10},{10,8},{12,... | collective-permute-start | bytes 393224 | tf_op jit(solution)/shard_map/ppermute | solution.py:28
  29.4 2.0 %collective-permute-done.8.refs_8_ = bf16[1,128,512]{2,1,0:T(8,128)(2,1)S(1)} collective-permute-done((bf16[1,128,512]{2,1,0:T(8,128)(2,1)}, bf16[1,128,512]{2,1,0:T(8,128)(2,1)S(1)}, u32[]{:S(2)}, u32[]{:S(2)}) %collective-permute-start.8) | collective-permute-done | bytes 131104 | tf_op jit(solution)/shard_map/ppermute | solution.py:28
  32.8 1.8 %tokens.1 = (bf16[2048,512]{1,0:T(8,128)(2,1)S(1)}, bf16[256,512]{1,0:T(8,128)(2,1)S(1)}) custom-call(s32[1]{0:T(128)} %bitcast.z_ref, s32[1]{0:T(128)} %bitcast.1.r_ref, bf16[256,2048]{1,0:T(8,128)(2,1)S(1)} %copy-done.5, bf16[512,512]{1,0:T(8,128)(2,1)S(1)} %broadcast_select_fusion.own_ref, bf16[1,256,512]{2,1,0:T(8,128)(2,1)S(1)} %collective-permute-done.refs_0_, ...), custom_call_target="tpu_custom_call" | custom-call | tf_op jit(solution)/shard_map/tokens/pallas_call | solution.py:97
  35.9 1.5 %collective-permute-done.9.other_ref = bf16[256,512]{1,0:T(8,128)(2,1)S(1)} collective-permute-done((bf16[256,512]{1,0:T(8,128)(2,1)S(1)}, bf16[256,512]{1,0:T(8,128)(2,1)S(1)}, u32[]{:S(2)}, u32[]{:S(2)}) %collective-permute-start.9) | collective-permute-done | bytes 262176 | tf_op jit(solution)/shard_map/ppermute | solution.py:28
  37.5 1.6 %terms.1 = bf16[4,4,32,1280]{3,2,1,0:T(8,128)(2,1)} custom-call(s32[1]{0:T(128)} %bitcast.2.t_ref, bf16[256,512]{1,0:T(8,128)(2,1)S(1)} %get-tuple-element.23.mine_ref, bf16[256,512]{1,0:T(8,128)(2,1)S(1)} %collective-permute-done.9.other_ref, bf16[256,1024]{1,0:T(8,128)(2,1)S(1)} %copy-done.7, bf16[256,256]{1,0:T(8,128)(2,1)S(1)} %copy-done.9), custom_call_target="tpu_custom_call" | custom-call | tf_op jit(solution)/shard_map/terms/pallas_call | solution.py:131
  39.1 3.5 %all-to-all-start = ((bf16[4,4,32,1280]{3,2,1,0:T(8,128)(2,1)}), bf16[4,4,32,1280]{3,2,1,0:T(8,128)(2,1)S(1)}, u32[]{:S(2)}, u32[]{:S(2)}) async-start(bf16[4,4,32,1280]{3,2,1,0:T(8,128)(2,1)} %terms.1), calls=%async_computation | async-start | bytes 2621440 | tf_op jit(solution)/shard_map/all_to_all | solution.py:32
  44.6 3.3 %collective-permute-start.15 = (bf16[1,256,1280]{2,1,0:T(8,128)(2,1)}, bf16[1,256,1280]{2,1,0:T(8,128)(2,1)}, u32[]{:S(2)}, u32[]{:S(2)}) collective-permute-start(bf16[1,256,1280]{2,1,0:T(8,128)(2,1)} %maximum_bitcast_fusion), channel_id=1, source_target_pairs={{0,16},{8,24},{16,0},{24,8},{1,17},{9,25},{17,1},{25,9},{2,18},{10... | collective-permute-start | bytes 1966088 | tf_op jit(solution)/shard_map/ppermute | solution.py:28
  47.9 11.8 %all-to-all-done.in_ref = bf16[4,4,32,1280]{3,2,1,0:T(8,128)(2,1)S(1)} async-done(((bf16[4,4,32,1280]{3,2,1,0:T(8,128)(2,1)}), bf16[4,4,32,1280]{3,2,1,0:T(8,128)(2,1)S(1)}, u32[]{:S(2)}, u32[]{:S(2)}) %all-to-all-start) | async-done | bytes 1310752 | tf_op jit(solution)/shard_map/all_to_all | solution.py:32
  60.5 5.7 %all-to-all-start.1 = ((bf16[4,32,1280]{2,1,0:T(8,128)(2,1)}), bf16[4,32,1280]{2,1,0:T(8,128)(2,1)S(1)}, u32[]{:S(2)}, u32[]{:S(2)}) async-start(bf16[4,32,1280]{2,1,0:T(8,128)(2,1)} %copy-done.4), calls=%async_computation.1 | async-start | bytes 655360 | tf_op jit(solution)/shard_map/all_to_all | solution.py:32
  66.3 2.0 %collective-permute-start.12 = (bf16[1,256,1280]{2,1,0:T(8,128)(2,1)}, bf16[1,256,1280]{2,1,0:T(8,128)(2,1)}, u32[]{:S(2)}, u32[]{:S(2)}) collective-permute-start(bf16[1,256,1280]{2,1,0:T(8,128)(2,1)} %maximum_bitcast_fusion), channel_id=1, source_target_pairs={{0,8},{8,0},{16,24},{24,16},{1,9},{9,1},{17,25},{25,17},{2,10},{10... | collective-permute-start | bytes 1966088 | tf_op jit(solution)/shard_map/ppermute | solution.py:28
  70.1 14.2 %all-to-all-done.1.got_ref = bf16[4,32,1280]{2,1,0:T(8,128)(2,1)S(1)} async-done(((bf16[4,32,1280]{2,1,0:T(8,128)(2,1)}), bf16[4,32,1280]{2,1,0:T(8,128)(2,1)S(1)}, u32[]{:S(2)}, u32[]{:S(2)}) %all-to-all-start.1) | async-done | bytes 327712 | tf_op jit(solution)/shard_map/all_to_all | solution.py:32
  85.2 4.8 %all-to-all-start.2 = ((bf16[4,32,1280]{2,1,0:T(8,128)(2,1)}), bf16[4,32,1280]{2,1,0:T(8,128)(2,1)S(1)}, u32[]{:S(2)}, u32[]{:S(2)}) async-start(bf16[4,32,1280]{2,1,0:T(8,128)(2,1)} %get-tuple-element.24), calls=%async_computation.2 | async-start | bytes 655360 | tf_op jit(solution)/shard_map/all_to_all | solution.py:32
  90.0 2.0 %collective-permute-start.18 = (bf16[1,256,1280]{2,1,0:T(8,128)(2,1)}, bf16[1,256,1280]{2,1,0:T(8,128)(2,1)}, u32[]{:S(2)}, u32[]{:S(2)}) collective-permute-start(bf16[1,256,1280]{2,1,0:T(8,128)(2,1)} %collective-permute-done.15.refs_3_), channel_id=1, source_target_pairs={{0,8},{8,0},{16,24},{24,16},{1,9},{9,1},{17,25},{25,17},{2,10},{10... | collective-permute-start | bytes 1966088 | tf_op jit(solution)/shard_map/ppermute | solution.py:28
  92.0 1.9 %fusion.1 = (bf16[1,128,1280]{2,1,0:T(8,128)(2,1)}, bf16[1,128,1280]{2,1,0:T(8,128)(2,1)}) fusion(bf16[1,256,1280]{2,1,0:T(8,128)(2,1)} %collective-permute-done.15.refs_3_), kind=kLoop, calls=%fused_computation.8 | loop fusion | bytes 1310720 | tf_op jit(solution)/shard_map/slice | solution.py:71
  94.0 1.7 %collective-permute-start.17 = (bf16[1,128,1280]{2,1,0:T(8,128)(2,1)}, bf16[1,128,1280]{2,1,0:T(8,128)(2,1)}, u32[]{:S(2)}, u32[]{:S(2)}) collective-permute-start(bf16[1,128,1280]{2,1,0:T(8,128)(2,1)} %get-tuple-element.40), channel_id=1, source_target_pairs={{0,4},{2,6},{4,0},{6,2},{1,5},{3,7},{5,1},{7,3},{8,12},{10,14},{12... | collective-permute-start | bytes 983048 | tf_op jit(solution)/shard_map/ppermute | solution.py:28
  97.1 4.7 %all-to-all-done.2.got_ref = bf16[4,32,1280]{2,1,0:T(8,128)(2,1)S(1)} async-done(((bf16[4,32,1280]{2,1,0:T(8,128)(2,1)}), bf16[4,32,1280]{2,1,0:T(8,128)(2,1)S(1)}, u32[]{:S(2)}, u32[]{:S(2)}) %all-to-all-start.2) | async-done | bytes 327712 | tf_op jit(solution)/shard_map/all_to_all | solution.py:32
  103.0 3.9 %all-to-all-start.3 = ((bf16[4,4,32,1280]{3,2,1,0:T(8,128)(2,1)}), bf16[4,4,32,1280]{3,2,1,0:T(8,128)(2,1)S(1)}, u32[]{:S(2)}, u32[]{:S(2)}) async-start(bf16[4,4,32,1280]{3,2,1,0:T(8,128)(2,1)} %plane.1), calls=%async_computation.3 | async-start | bytes 2621440 | tf_op jit(solution)/shard_map/all_to_all | solution.py:32
  106.9 1.9 %fusion.2 = (bf16[1,128,1280]{2,1,0:T(8,128)(2,1)}, bf16[1,128,1280]{2,1,0:T(8,128)(2,1)}) fusion(bf16[1,256,1280]{2,1,0:T(8,128)(2,1)} %collective-permute-done.12.refs_0_), kind=kLoop, calls=%fused_computation.9 | loop fusion | bytes 1310720 | tf_op jit(solution)/shard_map/slice | solution.py:71
  108.8 2.0 %collective-permute-start.14 = (bf16[1,128,1280]{2,1,0:T(8,128)(2,1)}, bf16[1,128,1280]{2,1,0:T(8,128)(2,1)}, u32[]{:S(2)}, u32[]{:S(2)}) collective-permute-start(bf16[1,128,1280]{2,1,0:T(8,128)(2,1)} %get-tuple-element.42), channel_id=1, source_target_pairs={{0,4},{2,6},{4,0},{6,2},{1,5},{3,7},{5,1},{7,3},{8,12},{10,14},{12... | collective-permute-start | bytes 983048 | tf_op jit(solution)/shard_map/ppermute | solution.py:28
  110.9 5.0 %collective-permute-done.18.refs_6_ = bf16[1,256,1280]{2,1,0:T(8,128)(2,1)} collective-permute-done((bf16[1,256,1280]{2,1,0:T(8,128)(2,1)}, bf16[1,256,1280]{2,1,0:T(8,128)(2,1)}, u32[]{:S(2)}, u32[]{:S(2)}) %collective-permute-start.18) | collective-permute-done | bytes 655392 | tf_op jit(solution)/shard_map/ppermute | solution.py:28
  115.9 1.7 %collective-permute-start.13 = (bf16[1,128,1280]{2,1,0:T(8,128)(2,1)}, bf16[1,128,1280]{2,1,0:T(8,128)(2,1)}, u32[]{:S(2)}, u32[]{:S(2)}) collective-permute-start(bf16[1,128,1280]{2,1,0:T(8,128)(2,1)} %get-tuple-element.43), channel_id=1, source_target_pairs={{0,2},{2,0},{4,6},{6,4},{1,3},{3,1},{5,7},{7,5},{8,10},{10,8},{12,... | collective-permute-start | bytes 983048 | tf_op jit(solution)/shard_map/ppermute | solution.py:28
  117.6 2.0 %fusion = (bf16[1,128,1280]{2,1,0:T(8,128)(2,1)}, bf16[1,128,1280]{2,1,0:T(8,128)(2,1)}) fusion(bf16[1,256,1280]{2,1,0:T(8,128)(2,1)} %collective-permute-done.18.refs_6_), kind=kLoop, calls=%fused_computation.7 | loop fusion | bytes 1310720 | tf_op jit(solution)/shard_map/slice | solution.py:71
  121.6 3.1 %all-to-all-done.3.got_ref = bf16[4,4,32,1280]{3,2,1,0:T(8,128)(2,1)S(1)} async-done(((bf16[4,4,32,1280]{3,2,1,0:T(8,128)(2,1)}), bf16[4,4,32,1280]{3,2,1,0:T(8,128)(2,1)S(1)}, u32[]{:S(2)}, u32[]{:S(2)}) %all-to-all-start.3) | async-done | bytes 1310752 | tf_op jit(solution)/shard_map/all_to_all | solution.py:32
  126.9 1.6 %directions.1 = (f32[2,128,1024]{2,1,0:T(8,128)}, f32[2,128,256]{2,1,0:T(8,128)}, bf16[512,1024]{1,0:T(8,128)(2,1)S(1)}, bf16[512,256]{1,0:T(8,128)(2,1)S(1)}, f32[16,128]{1,0:T(8,128)S(1)}) custom-call(s32[1]{0:T(128)} %bitcast.z_ref, bf16[4,4,32,1280]{3,2,1,0:T(8,128)(2,1)S(1)} %all-to-all-done.3.got_ref, f32[2,128,1024]{2,1,0:T(8,128)S(1)} %copy-done.3, ...), custom_call_target="tpu_custom_call" | custom-call | tf_op jit(solution)/shard_map/directions/pallas_call | solution.py:250
  128.5 3.1 %collective-permute-done.14.refs_2_ = bf16[1,128,1280]{2,1,0:T(8,128)(2,1)} collective-permute-done((bf16[1,128,1280]{2,1,0:T(8,128)(2,1)}, bf16[1,128,1280]{2,1,0:T(8,128)(2,1)}, u32[]{:S(2)}, u32[]{:S(2)}) %collective-permute-start.14) | collective-permute-done | bytes 327712 | tf_op jit(solution)/shard_map/ppermute | solution.py:28
  131.8 5.8 %collective-permute-done.20.refs_8_ = bf16[1,128,1280]{2,1,0:T(8,128)(2,1)} collective-permute-done((bf16[1,128,1280]{2,1,0:T(8,128)(2,1)}, bf16[1,128,1280]{2,1,0:T(8,128)(2,1)}, u32[]{:S(2)}, u32[]{:S(2)}) %collective-permute-start.20) | collective-permute-done | bytes 327712 | tf_op jit(solution)/shard_map/ppermute | solution.py:28
  137.7 8.4 %finish.1 = (f32[512,1024]{1,0:T(8,128)}, f32[512,256]{1,0:T(8,128)}, f32[512,1024]{1,0:T(8,128)}, f32[512,256]{1,0:T(8,128)}, bf16[2048,1024]{1,0:T(8,128)(2,1)}, /*index=5*/bf16[2048,256]{1,0:T(8,128)(2,1)}) custom-call(s32[1]{0:T(128)} %bitcast.z_ref, s32[1]{0:T(128)} %bitcast.1.r_ref, s32[1]{0:T(128)} %bitcast.2.t_ref, ...), custom_call_target="tpu_custom_call" | custom-call | tf_op jit(solution)/shard_map/finish/pallas_call | solution.py:393
  (58 shorter events, 23.4 us)
Async XLA Ops:
  0.6 32.1 %copy-start.5 = (bf16[256,2048]{1,0:T(8,128)(2,1)S(1)}, bf16[256,2048]{1,0:T(8,128)(2,1)}, u32[]{:S(2)}) copy-start(bf16[256,2048]{1,0:T(8,128)(2,1)} %x_ref.1) | copy-start | bytes 3145732
  1.9 16.2 %collective-permute-start.3 = (bf16[1,256,512]{2,1,0:T(8,128)(2,1)S(1)}, bf16[1,256,512]{2,1,0:T(8,128)(2,1)S(1)}, u32[]{:S(2)}, u32[]{:S(2)}) collective-permute-start(bf16[1,256,512]{2,1,0:T(8,128)(2,1)S(1)} %dynamic-slice_bitcast_fusion), channel_id=1, source_target_pairs={{0,16},{8,24},{16,0},{24,8},{1,17},{9,25},{17,1},{25,9},{2,18},{10... | collective-permute-start | bytes 786440 | tf_op jit(solution)/shard_map/ppermute | solution.py:28
  6.0 16.3 %collective-permute-start = (bf16[1,256,512]{2,1,0:T(8,128)(2,1)S(1)}, bf16[1,256,512]{2,1,0:T(8,128)(2,1)S(1)}, u32[]{:S(2)}, u32[]{:S(2)}) collective-permute-start(bf16[1,256,512]{2,1,0:T(8,128)(2,1)S(1)} %dynamic-slice_bitcast_fusion), channel_id=1, source_target_pairs={{0,8},{8,0},{16,24},{24,16},{1,9},{9,1},{17,25},{25,17},{2,10},{10... | collective-permute-start | bytes 786440 | tf_op jit(solution)/shard_map/ppermute | solution.py:28
  18.0 7.4 %collective-permute-start.6 = (bf16[1,256,512]{2,1,0:T(8,128)(2,1)S(1)}, bf16[1,256,512]{2,1,0:T(8,128)(2,1)S(1)}, u32[]{:S(2)}, u32[]{:S(2)}) collective-permute-start(bf16[1,256,512]{2,1,0:T(8,128)(2,1)S(1)} %collective-permute-done.3.refs_3_), channel_id=1, source_target_pairs={{0,8},{8,0},{16,24},{24,16},{1,9},{9,1},{17,25},{25,17},{2,10},{10... | collective-permute-start | bytes 786440 | tf_op jit(solution)/shard_map/ppermute | solution.py:28
  19.3 8.2 %collective-permute-start.5 = (bf16[1,128,512]{2,1,0:T(8,128)(2,1)S(1)}, bf16[1,128,512]{2,1,0:T(8,128)(2,1)S(1)}, u32[]{:S(2)}, u32[]{:S(2)}) collective-permute-start(bf16[1,128,512]{2,1,0:T(8,128)(2,1)S(1)} %get-tuple-element.46), channel_id=1, source_target_pairs={{0,4},{2,6},{4,0},{6,2},{1,5},{3,7},{5,1},{7,3},{8,12},{10,14},{12... | collective-permute-start | bytes 393224 | tf_op jit(solution)/shard_map/ppermute | solution.py:28
  20.9 16.6 %copy-start.7 = (bf16[256,1024]{1,0:T(8,128)(2,1)S(1)}, bf16[256,1024]{1,0:T(8,128)(2,1)}, u32[]{:S(2)}) copy-start(bf16[256,1024]{1,0:T(8,128)(2,1)} %cq_ref.1) | copy-start | bytes 1572868
  20.9 8.1 %collective-permute-start.4 = (bf16[1,128,512]{2,1,0:T(8,128)(2,1)}, bf16[1,128,512]{2,1,0:T(8,128)(2,1)S(1)}, u32[]{:S(2)}, u32[]{:S(2)}) collective-permute-start(bf16[1,128,512]{2,1,0:T(8,128)(2,1)} %get-tuple-element.47), channel_id=1, source_target_pairs={{0,2},{2,0},{4,6},{6,4},{1,3},{3,1},{5,7},{7,5},{8,10},{10,8},{12,... | collective-permute-start | bytes 393224 | tf_op jit(solution)/shard_map/ppermute | solution.py:28
  23.1 6.1 %collective-permute-start.2 = (bf16[1,128,512]{2,1,0:T(8,128)(2,1)}, bf16[1,128,512]{2,1,0:T(8,128)(2,1)S(1)}, u32[]{:S(2)}, u32[]{:S(2)}) collective-permute-start(bf16[1,128,512]{2,1,0:T(8,128)(2,1)} %get-tuple-element.48), channel_id=1, source_target_pairs={{0,4},{2,6},{4,0},{6,2},{1,5},{3,7},{5,1},{7,3},{8,12},{10,14},{12... | collective-permute-start | bytes 393224 | tf_op jit(solution)/shard_map/ppermute | solution.py:28
  23.6 5.8 %collective-permute-start.1 = (bf16[1,128,512]{2,1,0:T(8,128)(2,1)}, bf16[1,128,512]{2,1,0:T(8,128)(2,1)S(1)}, u32[]{:S(2)}, u32[]{:S(2)}) collective-permute-start(bf16[1,128,512]{2,1,0:T(8,128)(2,1)} %get-tuple-element.49), channel_id=1, source_target_pairs={{0,2},{2,0},{4,6},{6,4},{1,3},{3,1},{5,7},{7,5},{8,10},{10,8},{12,... | collective-permute-start | bytes 393224 | tf_op jit(solution)/shard_map/ppermute | solution.py:28
  26.2 5.2 %collective-permute-start.8 = (bf16[1,128,512]{2,1,0:T(8,128)(2,1)}, bf16[1,128,512]{2,1,0:T(8,128)(2,1)S(1)}, u32[]{:S(2)}, u32[]{:S(2)}) collective-permute-start(bf16[1,128,512]{2,1,0:T(8,128)(2,1)} %get-tuple-element.44), channel_id=1, source_target_pairs={{0,4},{2,6},{4,0},{6,2},{1,5},{3,7},{5,1},{7,3},{8,12},{10,14},{12... | collective-permute-start | bytes 393224 | tf_op jit(solution)/shard_map/ppermute | solution.py:28
  27.5 5.3 %collective-permute-start.7 = (bf16[1,128,512]{2,1,0:T(8,128)(2,1)}, bf16[1,128,512]{2,1,0:T(8,128)(2,1)}, u32[]{:S(2)}, u32[]{:S(2)}) collective-permute-start(bf16[1,128,512]{2,1,0:T(8,128)(2,1)} %get-tuple-element.45), channel_id=1, source_target_pairs={{0,2},{2,0},{4,6},{6,4},{1,3},{3,1},{5,7},{7,5},{8,10},{10,8},{12,... | collective-permute-start | bytes 393224 | tf_op jit(solution)/shard_map/ppermute | solution.py:28
  29.0 8.5 %copy-start.9 = (bf16[256,256]{1,0:T(8,128)(2,1)S(1)}, bf16[256,256]{1,0:T(8,128)(2,1)}, u32[]{:S(2)}) copy-start(bf16[256,256]{1,0:T(8,128)(2,1)} %ck_ref.1) | copy-start | bytes 393220
  34.6 1.3 copy-start.1
  35.9 1.5 %collective-permute-start.9 = (bf16[256,512]{1,0:T(8,128)(2,1)S(1)}, bf16[256,512]{1,0:T(8,128)(2,1)S(1)}, u32[]{:S(2)}, u32[]{:S(2)}) collective-permute-start(bf16[256,512]{1,0:T(8,128)(2,1)S(1)} %get-tuple-element.23.mine_ref), channel_id=1, source_target_pairs={{0,1},{1,0},{2,3},{3,2},{4,5},{5,4},{6,7},{7,6},{8,9},{9,8},{10,11... | collective-permute-start | bytes 786440 | tf_op jit(solution)/shard_map/ppermute | solution.py:28
  37.5 6.2 %copy-start = (f32[512,1024]{1,0:T(8,128)S(1)}, f32[512,1024]{1,0:T(8,128)}, u32[]{:S(2)}) copy-start(f32[512,1024]{1,0:T(8,128)} %wq_ref.1) | copy-start | bytes 6291460
  39.1 20.5 %all-to-all-start = ((bf16[4,4,32,1280]{3,2,1,0:T(8,128)(2,1)}), bf16[4,4,32,1280]{3,2,1,0:T(8,128)(2,1)S(1)}, u32[]{:S(2)}, u32[]{:S(2)}) async-start(bf16[4,4,32,1280]{3,2,1,0:T(8,128)(2,1)} %terms.1), calls=%async_computation | async-start | bytes 2621440 | tf_op jit(solution)/shard_map/all_to_all | solution.py:32
  44.6 45.4 %collective-permute-start.15 = (bf16[1,256,1280]{2,1,0:T(8,128)(2,1)}, bf16[1,256,1280]{2,1,0:T(8,128)(2,1)}, u32[]{:S(2)}, u32[]{:S(2)}) collective-permute-start(bf16[1,256,1280]{2,1,0:T(8,128)(2,1)} %maximum_bitcast_fusion), channel_id=1, source_target_pairs={{0,16},{8,24},{16,0},{24,8},{1,17},{9,25},{17,1},{25,9},{2,18},{10... | collective-permute-start | bytes 1966088 | tf_op jit(solution)/shard_map/ppermute | solution.py:28
  60.5 23.8 %all-to-all-start.1 = ((bf16[4,32,1280]{2,1,0:T(8,128)(2,1)}), bf16[4,32,1280]{2,1,0:T(8,128)(2,1)S(1)}, u32[]{:S(2)}, u32[]{:S(2)}) async-start(bf16[4,32,1280]{2,1,0:T(8,128)(2,1)} %copy-done.4), calls=%async_computation.1 | async-start | bytes 655360 | tf_op jit(solution)/shard_map/all_to_all | solution.py:32
  66.3 71.4 %collective-permute-start.11 = (bf16[2048,512]{1,0:T(8,128)(2,1)}, bf16[2048,512]{1,0:T(8,128)(2,1)}, u32[]{:S(2)}, u32[]{:S(2)}) collective-permute-start(bf16[2048,512]{1,0:T(8,128)(2,1)} %copy-done.1), channel_id=1, source_target_pairs={{0,1},{1,0},{2,3},{3,2},{4,5},{5,4},{6,7},{7,6},{8,9},{9,8},{10,11... | collective-permute-start | bytes 6291464 | tf_op jit(solution)/shard_map/ppermute | solution.py:28
  66.3 40.6 %collective-permute-start.12 = (bf16[1,256,1280]{2,1,0:T(8,128)(2,1)}, bf16[1,256,1280]{2,1,0:T(8,128)(2,1)}, u32[]{:S(2)}, u32[]{:S(2)}) collective-permute-start(bf16[1,256,1280]{2,1,0:T(8,128)(2,1)} %maximum_bitcast_fusion), channel_id=1, source_target_pairs={{0,8},{8,0},{16,24},{24,16},{1,9},{9,1},{17,25},{25,17},{2,10},{10... | collective-permute-start | bytes 1966088 | tf_op jit(solution)/shard_map/ppermute | solution.py:28
  85.2 16.6 %all-to-all-start.2 = ((bf16[4,32,1280]{2,1,0:T(8,128)(2,1)}), bf16[4,32,1280]{2,1,0:T(8,128)(2,1)S(1)}, u32[]{:S(2)}, u32[]{:S(2)}) async-start(bf16[4,32,1280]{2,1,0:T(8,128)(2,1)} %get-tuple-element.24), calls=%async_computation.2 | async-start | bytes 655360 | tf_op jit(solution)/shard_map/all_to_all | solution.py:32
  90.0 25.9 %collective-permute-start.18 = (bf16[1,256,1280]{2,1,0:T(8,128)(2,1)}, bf16[1,256,1280]{2,1,0:T(8,128)(2,1)}, u32[]{:S(2)}, u32[]{:S(2)}) collective-permute-start(bf16[1,256,1280]{2,1,0:T(8,128)(2,1)} %collective-permute-done.15.refs_3_), channel_id=1, source_target_pairs={{0,8},{8,0},{16,24},{24,16},{1,9},{9,1},{17,25},{25,17},{2,10},{10... | collective-permute-start | bytes 1966088 | tf_op jit(solution)/shard_map/ppermute | solution.py:28
  94.0 25.6 %collective-permute-start.17 = (bf16[1,128,1280]{2,1,0:T(8,128)(2,1)}, bf16[1,128,1280]{2,1,0:T(8,128)(2,1)}, u32[]{:S(2)}, u32[]{:S(2)}) collective-permute-start(bf16[1,128,1280]{2,1,0:T(8,128)(2,1)} %get-tuple-element.40), channel_id=1, source_target_pairs={{0,4},{2,6},{4,0},{6,2},{1,5},{3,7},{5,1},{7,3},{8,12},{10,14},{12... | collective-permute-start | bytes 983048 | tf_op jit(solution)/shard_map/ppermute | solution.py:28
  95.7 25.4 %collective-permute-start.16 = (bf16[1,128,1280]{2,1,0:T(8,128)(2,1)}, bf16[1,128,1280]{2,1,0:T(8,128)(2,1)}, u32[]{:S(2)}, u32[]{:S(2)}) collective-permute-start(bf16[1,128,1280]{2,1,0:T(8,128)(2,1)} %get-tuple-element.41), channel_id=1, source_target_pairs={{0,2},{2,0},{4,6},{6,4},{1,3},{3,1},{5,7},{7,5},{8,10},{10,8},{12,... | collective-permute-start | bytes 983048 | tf_op jit(solution)/shard_map/ppermute | solution.py:28
  103.0 21.7 %all-to-all-start.3 = ((bf16[4,4,32,1280]{3,2,1,0:T(8,128)(2,1)}), bf16[4,4,32,1280]{3,2,1,0:T(8,128)(2,1)S(1)}, u32[]{:S(2)}, u32[]{:S(2)}) async-start(bf16[4,4,32,1280]{3,2,1,0:T(8,128)(2,1)} %plane.1), calls=%async_computation.3 | async-start | bytes 2621440 | tf_op jit(solution)/shard_map/all_to_all | solution.py:32
  108.8 22.8 %collective-permute-start.14 = (bf16[1,128,1280]{2,1,0:T(8,128)(2,1)}, bf16[1,128,1280]{2,1,0:T(8,128)(2,1)}, u32[]{:S(2)}, u32[]{:S(2)}) collective-permute-start(bf16[1,128,1280]{2,1,0:T(8,128)(2,1)} %get-tuple-element.42), channel_id=1, source_target_pairs={{0,4},{2,6},{4,0},{6,2},{1,5},{3,7},{5,1},{7,3},{8,12},{10,14},{12... | collective-permute-start | bytes 983048 | tf_op jit(solution)/shard_map/ppermute | solution.py:28
  115.9 15.9 %collective-permute-start.13 = (bf16[1,128,1280]{2,1,0:T(8,128)(2,1)}, bf16[1,128,1280]{2,1,0:T(8,128)(2,1)}, u32[]{:S(2)}, u32[]{:S(2)}) collective-permute-start(bf16[1,128,1280]{2,1,0:T(8,128)(2,1)} %get-tuple-element.43), channel_id=1, source_target_pairs={{0,2},{2,0},{4,6},{6,4},{1,3},{3,1},{5,7},{7,5},{8,10},{10,8},{12,... | collective-permute-start | bytes 983048 | tf_op jit(solution)/shard_map/ppermute | solution.py:28
  119.6 18.1 %collective-permute-start.20 = (bf16[1,128,1280]{2,1,0:T(8,128)(2,1)}, bf16[1,128,1280]{2,1,0:T(8,128)(2,1)}, u32[]{:S(2)}, u32[]{:S(2)}) collective-permute-start(bf16[1,128,1280]{2,1,0:T(8,128)(2,1)} %get-tuple-element.38), channel_id=1, source_target_pairs={{0,4},{2,6},{4,0},{6,2},{1,5},{3,7},{5,1},{7,3},{8,12},{10,14},{12... | collective-permute-start | bytes 983048 | tf_op jit(solution)/shard_map/ppermute | solution.py:28
  121.0 16.7 %collective-permute-start.19 = (bf16[1,128,1280]{2,1,0:T(8,128)(2,1)}, bf16[1,128,1280]{2,1,0:T(8,128)(2,1)}, u32[]{:S(2)}, u32[]{:S(2)}) collective-permute-start(bf16[1,128,1280]{2,1,0:T(8,128)(2,1)} %get-tuple-element.39), channel_id=1, source_target_pairs={{0,2},{2,0},{4,6},{6,4},{1,3},{3,1},{5,7},{7,5},{8,10},{10,8},{12,... | collective-permute-start | bytes 983048 | tf_op jit(solution)/shard_map/ppermute | solution.py:28
  126.9 10.8 %copy-start.2 = (bf16[2048,512]{1,0:T(8,128)(2,1)S(1)}, bf16[2048,512]{1,0:T(8,128)(2,1)}, u32[]{:S(2)}) copy-start(bf16[2048,512]{1,0:T(8,128)(2,1)} %copy-done.1) | copy-start | bytes 6291460
  126.9 10.8 %copy-start.6 = (f32[512,256]{1,0:T(8,128)S(1)}, f32[512,256]{1,0:T(8,128)}, u32[]{:S(2)}) copy-start(f32[512,256]{1,0:T(8,128)} %wk_ref.1) | copy-start | bytes 1572868
  131.6 6.1 %collective-permute-start.10 = (f32[16,128]{1,0:T(8,128)S(1)}, f32[16,128]{1,0:T(8,128)S(1)}, u32[]{:S(2)}, u32[]{:S(2)}) collective-permute-start(f32[16,128]{1,0:T(8,128)S(1)} %get-tuple-element.26.sums_ref), channel_id=1, source_target_pairs={{0,1},{1,0},{2,3},{3,2},{4,5},{5,4},{6,7},{7,6},{8,9},{9,8},{10,11... | collective-permute-start | bytes 24584 | tf_op jit(solution)/shard_map/ppermute | solution.py:28
  (3 other events, 2.9 us)

commit v2 on v1

v2 whole, which is shorter than its diff:
```python
import functools

import jax
import jax.numpy as jnp
from jax import lax
from jax.experimental import pallas as pl
from jax.experimental.pallas import tpu as pltpu
from jax.sharding import PartitionSpec as P


BF = jnp.bfloat16
F32 = jnp.float32
SMALL = pltpu.CompilerParams(vmem_limit_bytes=12 * 2**20)
LARGE = pltpu.CompilerParams(vmem_limit_bytes=28 * 2**20)


def whole(a):
    shape = getattr(a, "shape", a)
    return pl.BlockSpec(tuple(shape), lambda *_: (0,) * len(shape))


in_space = pltpu.with_memory_space_constraint


def contract(left, right):
    return lax.dot_general(left, right, (((0,), (0,)), ((), ())), preferred_element_type=F32)


def xor_swap(value, axis, bit):
    size = lax.axis_size(axis)
    return lax.ppermute(value, axis, [(i, i ^ bit) for i in range(size)])


def exchange(value, axis):
    return lax.all_to_all(value, axis, 0, 0, tiled=True)


def spread(own):
    own = own[None]
    rest, rels = None, []
    bit = lax.axis_size("fs") // 2
    while bit:
        near = xor_swap(own, "fs", bit)
        if rest is None:
            rest, rels = near, [bit]
        elif bit > 1:
            far = xor_swap(rest, "fs", bit)
            rest = jnp.concatenate([rest, near, far], axis=0)
            rels = rels + [bit] + [i ^ bit for i in rels]
        else:
            far = xor_swap(rest, "fs", bit)
            return [([bit], near), (rels, rest), ([i ^ bit for i in rels], far)]
        bit //= 2
    return [(rels, rest)]


def parity(r):
    return jnp.bitwise_xor(jnp.bitwise_and(r, 1), jnp.right_shift(r, 1))


def share(r):
    return (2 * parity(r), 2) if lax.axis_size("rep") == 4 else (r, 1)


def spread_planes(own):
    n_r = lax.axis_size("rep")
    pieces = []
    for m, part in enumerate(own):
        for n, (rels, got) in enumerate(spread(part)):
            pieces.append((rels, got, lambda r, m=m: share(r)[0] + m, n))
            if n_r != 4:
                for i in range(1, n_r):
                    near = xor_swap(got, "rep", i)
                    pieces.append((rels, near, lambda r, i=i: jnp.bitwise_xor(r, i), n))
            elif len(own) == 2:
                near = xor_swap(got, "rep", 1 + m)
                pieces.append((rels, near, lambda r, m=m: 2 + m - 2 * parity(r), n))
            else:
                h = got.shape[1] // 2
                for i, half in enumerate((got[:, :h], got[:, h:])):
                    near = xor_swap(half, "rep", 1 + i)
                    pieces.append((rels, near, lambda r, i=i: 2 + i - 2 * parity(r), n))
    return pieces


def spread_basis(basis_q, basis_k, r, t):
    n_f, n_r = lax.axis_size("fs"), lax.axis_size("rep")
    h = basis_q.shape[0] // n_r

    def rows(first, count):
        mine = (lax.dynamic_slice_in_dim(b, first * h, count * h, 0) for b in (basis_q, basis_k))
        return jnp.where(t == 0, *mine)

    first, count = share(r)
    if n_f != 4 or n_r != 4:
        return spread_planes([rows(first, count)])
    two = xor_swap(rows(r, 1)[None], "fs", 2)
    one = xor_swap(rows(first, count)[None], "fs", 1)
    three = xor_swap(two, "fs", 1)
    pieces = [([1], one, lambda r: share(r)[0], 0)]
    for i, half in enumerate((one[:, :h], one[:, h:])):
        near = xor_swap(half, "rep", 1 + i)
        pieces.append(([1], near, lambda r, i=i: 2 + i - 2 * parity(r), 0))
    for rel, got in ((2, two), (3, three)):
        pieces.append(([rel], got, lambda r: r, rel - 1))
        for i in range(1, n_r):
            near = xor_swap(got, "rep", i)
            pieces.append(([rel], near, lambda r, i=i: jnp.bitwise_xor(r, i), rel - 1))
    return pieces


def token_kernel(rels, z_ref, r_ref, t_ref, x_ref, own_q_ref, own_k_ref, *refs):
    parts, (basis_ref, token_ref) = refs[: len(rels)], refs[len(rels) : len(rels) + 2]
    x_vmem, basis_vmem, x_sem, own_sem, sems, out_sem = refs[len(rels) + 2 :]
    x_load = pltpu.make_async_copy(x_ref, x_vmem, x_sem)
    x_load.start()
    z = z_ref[0]
    rows = own_q_ref.shape[0]
    own_at = pl.ds(pl.multiple_of(z * rows, rows), rows)
    for query, source in ((True, own_q_ref), (False, own_k_ref)):

        @pl.when((t_ref[0] == 0) == query)
        def _():
            pltpu.make_async_copy(source, basis_vmem.at[own_at], own_sem).start()

    loads = []
    for n, ((rel, first), part) in enumerate(zip(rels, parts)):
        for j, rel_j in enumerate(rel):
            at = jnp.bitwise_xor(z, rel_j) * rows + first(r_ref[0]) * (rows // lax.axis_size("rep"))
            at = pl.ds(pl.multiple_of(at, 16), part.shape[1])
            loads.append(pltpu.make_async_copy(part.at[j], basis_vmem.at[at], sems.at[n, j]))
            loads[-1].start()
    x_load.wait()
    pltpu.make_async_copy(own_q_ref, basis_vmem.at[own_at], own_sem).wait()
    for load in loads:
        load.wait()
    store = pltpu.make_async_copy(basis_vmem, basis_ref, out_sem)
    store.start()
    token_ref[...] = jnp.dot(x_vmem[...], basis_vmem[...], preferred_element_type=F32).astype(BF)
    store.wait()


def tokens(z, r, t, x, own_q, own_k, parts):
    shape = (x.shape[1], own_q.shape[1])
    hbm = pl.BlockSpec(memory_space=pltpu.HBM)
    token = (x.shape[0], own_q.shape[1])
    sources = (x, own_q, own_k, *[p for _, p, _, _ in parts])
    return pl.pallas_call(
        functools.partial(token_kernel, tuple((tuple(rel), first) for rel, _, first, _ in parts)),
        in_specs=[pl.BlockSpec(memory_space=pltpu.SMEM)] * 3 + [hbm] * len(sources),
        out_specs=[hbm, whole(token)],
        grid=(1,),
        out_shape=[pltpu.HBM(shape, BF), pltpu.VMEM(token, BF)],
        scratch_shapes=[
            pltpu.VMEM(x.shape, BF),
            pltpu.VMEM(shape, BF),
            pltpu.SemaphoreType.DMA,
            pltpu.SemaphoreType.DMA,
            pltpu.SemaphoreType.DMA((len(parts), max(len(rel) for rel, _, _, _ in parts))),
            pltpu.SemaphoreType.DMA,
        ],
        compiler_params=SMALL,
        name="tokens",
    )(z, r, t, *[in_space(a, pltpu.HBM) for a in sources[:3]], *sources[3:])


def terms_kernel(t_ref, mine_ref, other_ref, cq_ref, ck_ref, out_ref):
    n_r, n_f, rows, _ = out_ref.shape
    cols_q = cq_ref.shape[1]
    query_mine = t_ref[0] == 0
    mine, other = mine_ref[...], other_ref[...]
    q = contract(jnp.where(query_mine, mine, other), cq_ref[...]).astype(BF)
    k = contract(jnp.where(query_mine, other, mine), ck_ref[...]).astype(BF)
    for j in range(n_f):
        for i in range(n_r):
            at = (j * n_r + i) * rows
            out_ref[i, j, :, :cols_q] = q[at : at + rows]
            out_ref[i, j, :, cols_q:] = k[at : at + rows]


def terms(t, mine, other, cot_q, cot_k):
    n_f, n_r = lax.axis_size("fs"), lax.axis_size("rep")
    shape = (n_r, n_f, mine.shape[1] // (n_f * n_r), cot_q.shape[1] + cot_k.shape[1])
    return pl.pallas_call(
        terms_kernel,
        in_specs=[pl.BlockSpec(memory_space=pltpu.SMEM)]
        + [whole(a) for a in (mine, other, cot_q, cot_k)],
        out_specs=whole(shape),
        grid=(1,),
        out_shape=pltpu.HBM(shape, BF),
        compiler_params=SMALL,
        name="terms",
    )(t, mine, other, cot_q, cot_k)


def sum_kernel(in_ref, out_ref):
    total = in_ref[0].astype(F32)
    for i in range(1, in_ref.shape[0]):
        total = total + in_ref[i].astype(F32)
    out_ref[...] = total.astype(BF)


def sum_first(value):
    return pl.pallas_call(
        sum_kernel,
        in_specs=[whole(value)],
        out_specs=whole(value.shape[1:]),
        grid=(1,),
        out_shape=pltpu.HBM(value.shape[1:], BF),
        compiler_params=SMALL,
        name="sum_first",
    )(value)


def moment_update(first, second, low):
    first = 0.9 * first + 0.1 * low
    second = 0.95 * second + 0.05 * low * low
    return first, second, first / (jnp.sqrt(second) + 1e-08)


def piece_kernel(got_ref, mq_ref, mk_ref, low_ref, out_ref):
    cols_q = mq_ref.shape[2]
    total = got_ref[0].astype(F32)
    for i in range(1, got_ref.shape[0]):
        total = total + got_ref[i].astype(F32)
    low = total.astype(BF)
    low_ref[...] = low
    low = low.astype(F32)
    q = moment_update(mq_ref[0], mq_ref[1], low[:, :cols_q])[2].astype(BF)
    k = moment_update(mk_ref[0], mk_ref[1], low[:, cols_q:])[2].astype(BF)
    for i in range(out_ref.shape[0]):
        out_ref[i, :, :cols_q] = q
        out_ref[i, :, cols_q:] = k


def piece(r, got, moments_q, moments_k):
    n_f, rows, cols = got.shape
    moments_q = lax.dynamic_slice_in_dim(moments_q, r * rows, rows, 1)
    moments_k = lax.dynamic_slice_in_dim(moments_k, r * rows, rows, 1)
    return pl.pallas_call(
        piece_kernel,
        in_specs=[whole(got), whole(moments_q), whole(moments_k)],
        out_specs=[whole((rows, cols)), whole((n_f, rows, cols))],
        grid=(1,),
        out_shape=[
            jax.ShapeDtypeStruct((rows, cols), BF),
            pltpu.HBM((n_f, rows, cols), BF),
        ],
        compiler_params=SMALL,
        name="piece",
    )(got, moments_q, moments_k)


def plane_kernel(z_ref, got_ref, low_ref, out_ref):
    for i in range(out_ref.shape[0]):
        out_ref[i] = got_ref[...]
        out_ref[i, z_ref[0]] = low_ref[...]


def plane(z, got, low):
    return pl.pallas_call(
        plane_kernel,
        in_specs=[pl.BlockSpec(memory_space=pltpu.SMEM), whole(got), whole(low)],
        out_specs=whole((lax.axis_size("rep"), *got.shape)),
        grid=(1,),
        out_shape=jax.ShapeDtypeStruct((lax.axis_size("rep"), *got.shape), BF),
        compiler_params=SMALL,
        name="plane",
    )(z, got, low)


def squares(value):
    rows, cols = value.shape
    total = jnp.sum(jnp.square(value).reshape(rows // 8, 8, cols), axis=0)
    parts = [total[:, i : i + 128] for i in range(0, cols, 128)]
    return functools.reduce(jnp.add, parts)


def directions_kernel(z_ref, got_ref, mq_ref, mk_ref, nq_ref, nk_ref, dq_ref, dk_ref, sums_ref):
    n_r, n_f, rows, _ = got_ref.shape
    cols_q = mq_ref.shape[2]
    z = z_ref[0]
    own = n_r * rows
    for j in range(n_f):
        got = jnp.concatenate([got_ref[i, j] for i in range(n_r)], axis=0)
        dq_ref[j * own : (j + 1) * own, :] = got[:, :cols_q]
        dk_ref[j * own : (j + 1) * own, :] = got[:, cols_q:]
    low = jnp.concatenate([got_ref[i, z] for i in range(n_r)], axis=0).astype(F32)
    q = moment_update(mq_ref[0], mq_ref[1], low[:, :cols_q])
    k = moment_update(mk_ref[0], mk_ref[1], low[:, cols_q:])
    nq_ref[0], nq_ref[1] = q[0], q[1]
    nk_ref[0], nk_ref[1] = k[0], k[1]
    at = pl.ds(pl.multiple_of(z * own, own), own)
    dq_ref[at, :] = q[2].astype(BF)
    dk_ref[at, :] = k[2].astype(BF)
    sums_ref[:8, :] = squares(dq_ref[...].astype(F32))
    sums_ref[8:, :] = squares(dk_ref[...].astype(F32))


def directions(z, got, moments_q, moments_k):
    n_r, n_f, rows, _ = got.shape
    rank = n_r * n_f * rows
    return pl.pallas_call(
        directions_kernel,
        in_specs=[pl.BlockSpec(memory_space=pltpu.SMEM), whole(got), whole(moments_q), whole(moments_k)],
        out_specs=[
            whole(moments_q),
            whole(moments_k),
            whole((rank, moments_q.shape[2])),
            whole((rank, moments_k.shape[2])),
            whole((16, 128)),
        ],
        grid=(1,),
        out_shape=[
            jax.ShapeDtypeStruct(moments_q.shape, F32),
            jax.ShapeDtypeStruct(moments_k.shape, F32),
            pltpu.VMEM((rank, moments_q.shape[2]), BF),
            pltpu.VMEM((rank, moments_k.shape[2]), BF),
            pltpu.VMEM((16, 128), F32),
        ],
        compiler_params=SMALL,
        name="directions",
    )(z, got, moments_q, moments_k)


def gather_pieces(plan, slots, rel, r, pieces, to, sems):
    loads = []
    h = to.shape[1] // lax.axis_size("rep")
    for i, (rels, first) in enumerate(plan):
        if rel in rels:
            j = rels.index(rel)
            at = pl.ds(pl.multiple_of(first(r) * h, 16), pieces[i].shape[1])
            loads.append(
                pltpu.make_async_copy(pieces[i].at[j], to.at[slots[rel], at], sems.at[i, j])
            )
            loads[-1].start()
    return loads


def slots_of(plan):
    rels = []
    for got, _ in plan:
        rels += [rel for rel in got if rel not in rels]
    return {rel: i for i, rel in enumerate(rels)}


def plan_of(pieces):
    return tuple((tuple(rels), first) for rels, _, first, _ in pieces)


def semaphores(plan):
    return pltpu.SemaphoreType.DMA((len(plan), max(len(rels) for rels, _ in plan)))


CHUNK = 256


def finish_kernel(
    plan, n_tp, z_ref, r_ref, t_ref, sums_ref, other_sums_ref, dq_ref, dk_ref,
    mine_ref, other_ref, wq_ref, wk_ref, *refs,
):
    n = len(plan)
    pieces, outs, results, copies_out = refs[:n], refs[n : n + 6], refs[n + 6 : n + 10], refs[n + 10 : n + 12]
    bases, weights, (last, basis_sem, weight_sem, out_sem, copy_sem, sems) = (
        refs[n + 12 : n + 14], refs[n + 14 : n + 16], refs[n + 16 :]
    )
    z = z_ref[0]
    rows, cols_q = wq_ref.shape
    cols_k = wk_ref.shape[1]
    rank = dq_ref.shape[0]
    slots = slots_of(plan)
    order = [*slots]
    order = [order[0], 0, *order[1:]]

    def block(rel):
        return pl.ds(pl.multiple_of(jnp.bitwise_xor(z, rel) * rows, rows), rows)

    loads = {}
    weight_loads = [
        pltpu.make_async_copy(source, to, weight_sem.at[i])
        for i, (source, to) in enumerate(zip((wq_ref, wk_ref), weights))
    ]
    for step, rel in enumerate(order):
        for query in (True, False):

            @pl.when((t_ref[0] == 0) == query)
            def _():
                for mat, source in enumerate((mine_ref, other_ref) if query else (other_ref, mine_ref)):
                    pltpu.make_async_copy(
                        source.at[block(rel)], bases[mat].at[step], basis_sem.at[mat, step]
                    ).start()

        if rel == 0:
            for load in weight_loads:
                load.start()
        else:
            loads[rel] = gather_pieces(plan, slots, rel, r_ref[0], pieces, last, sems)

    def scale(at, cols):
        total = jnp.sum(sums_ref[at, :] + other_sums_ref[at, :], keepdims=True)
        return lax.rsqrt(total / (rank * cols * n_tp) + 1e-06)

    scales = scale(slice(0, 8), cols_q), scale(slice(8, 16), cols_k)
    directions = dq_ref, dk_ref
    stores = []

    def store(source, to, sem):
        stores.append(pltpu.make_async_copy(source, to, sem))
        stores[-1].start()

    for step, rel in enumerate(order):
        for load in loads.get(rel, []):
            load.wait()
        for mat, part in ((0, slice(0, cols_q)), (1, slice(cols_q, cols_q + cols_k))):
            pltpu.make_async_copy(
                mine_ref.at[block(rel)], bases[mat].at[step], basis_sem.at[mat, step]
            ).wait()
            if rel == 0:
                weight_loads[mat].wait()
            for top in range(0, rows, CHUNK):
                at = slice(top, min(rows, top + CHUNK))
                product = jnp.dot(
                    bases[mat][step, at], directions[mat][...], preferred_element_type=F32
                )
                if rel == 0:
                    product = scales[mat] * product
                    results[mat][at] = product
                    new = weights[mat][at] - 0.02 * product
                    results[2 + mat][at] = new
                else:
                    old = last[slots[rel], at, part]
                    new = old.astype(F32) - (0.02 * scales[mat]) * product
                copies_out[mat][step, at] = new.astype(BF)
            if rel == 0:
                store(results[mat], outs[mat], out_sem.at[mat])
                store(results[2 + mat], outs[2 + mat], out_sem.at[2 + mat])
            store(copies_out[mat].at[step], outs[4 + mat].at[block(rel)], copy_sem.at[mat, step])
    for one in stores:
        one.wait()


def finish(z, r, t, sums, other_sums, dir_q, dir_k, mine, other, weight_q, weight_k, pieces):
    n_f, n_tp = lax.axis_size("fs"), lax.axis_size("tp")
    rows, cols_q = weight_q.shape
    cols_k = weight_k.shape[1]
    rank = mine.shape[1]
    plan = plan_of(pieces)
    hbm = pl.BlockSpec(memory_space=pltpu.HBM)
    smem = pl.BlockSpec(memory_space=pltpu.SMEM)
    vmem = pl.BlockSpec(memory_space=pltpu.VMEM)
    shapes = [
        ((rows, cols_q), F32),
        ((rows, cols_k), F32),
        ((rows, cols_q), F32),
        ((rows, cols_k), F32),
        ((rows * n_f, cols_q), BF),
        ((rows * n_f, cols_k), BF),
    ]
    inside = [in_space(a, pltpu.VMEM) for a in (sums, other_sums, dir_q, dir_k)]
    outside = [
        in_space(a, pltpu.HBM) for a in (mine, other, weight_q, weight_k, *[p[1] for p in pieces])
    ]
    return pl.pallas_call(
        functools.partial(finish_kernel, plan, n_tp),
        in_specs=[smem] * 3 + [vmem] * len(inside) + [hbm] * len(outside),
        out_specs=[hbm] * 6,
        out_shape=[pltpu.HBM(*s) for s in shapes],
        scratch_shapes=[
            *[pltpu.VMEM(*s) for s in shapes[:4]],
            pltpu.VMEM((n_f, rows, cols_q), BF),
            pltpu.VMEM((n_f, rows, cols_k), BF),
            *[pltpu.VMEM((n_f, rows, rank), BF)] * 2,
            pltpu.VMEM((rows, cols_q), F32),
            pltpu.VMEM((rows, cols_k), F32),
            pltpu.VMEM((len(slots_of(plan)), rows, cols_q + cols_k), BF),
            pltpu.SemaphoreType.DMA((2, n_f)),
            pltpu.SemaphoreType.DMA((2,)),
            pltpu.SemaphoreType.DMA((4,)),
            pltpu.SemaphoreType.DMA((2, n_f)),
            semaphores(plan),
        ],
        compiler_params=LARGE,
        name="finish",
    )(z, r, t, *inside, *outside)


def on_device(
    inputs,
    cot_query,
    cot_key,
    basis_query,
    basis_key,
    weight_query,
    weight_key,
    moments_query,
    moments_key,
):
    n_r = lax.axis_size("rep")
    z, r, t = lax.axis_index("fs"), lax.axis_index("rep"), lax.axis_index("tp")
    own_rows, _ = basis_query.shape
    h = own_rows // n_r
    at_z, at_r, at_t = (i.astype(jnp.int32)[None] for i in (z, r, t))
    first, count = share(r)

    parts = spread_basis(basis_query, basis_key, r, t)

    mine = [
        jnp.concatenate(
            [
                lax.dynamic_slice_in_dim(w, (first + i) * h, h, 0).astype(BF)
                for w in (weight_query, weight_key)
            ],
            axis=1,
        )
        for i in range(count)
    ]
    pieces = spread_planes(mine)

    basis, token = tokens(at_z, at_r, at_t, inputs, basis_query, basis_key, parts)
    other_token = xor_swap(token, "tp", 1)
    other_basis = xor_swap(basis, "tp", 1)
    low = exchange(terms(at_t, token, other_token, cot_query, cot_key), "rep")
    low = exchange(sum_first(low), "fs")
    low, rows = piece(r, low, moments_query, moments_key)
    rows = plane(at_z, exchange(rows, "fs"), low)
    rows = exchange(rows, "rep")
    new_q, new_k, dir_q, dir_k, sums = directions(at_z, rows, moments_query, moments_key)
    other_sums = xor_swap(sums, "tp", 1)
    outs = finish(
        at_z, at_r, at_t, sums, other_sums, dir_q, dir_k,
        basis, other_basis, weight_query, weight_key, pieces,
    )
    return (*outs, new_q, new_k)


def solution(mesh):
    in_specs = (
        P(("fs", "rep"), None),
        P(("fs", "rep"), "tp"),
        P(("fs", "rep"), "tp"),
        P("fs", None),
        P("fs", None),
        P("fs", "tp"),
        P("fs", "tp"),
        P(None, "fs", "tp"),
        P(None, "fs", "tp"),
    )
    out_specs = (
        P("fs", "tp"),
        P("fs", "tp"),
        P("fs", "tp"),
        P("fs", "tp"),
        P(None, "tp"),
        P(None, "tp"),
        P(None, "fs", "tp"),
        P(None, "fs", "tp"),
    )

    return jax.shard_map(
        on_device, mesh=mesh, in_specs=in_specs, out_specs=out_specs, check_vma=False
    )
```

time: 147 us -> 154 us (1.048)
  blocking collectives: 0 us -> 21.2 us
  local copies, waits for them, and re-layouts: 15.1 us -> 2.98 us
  starting transfers between devices: 47.3 us -> 42.2 us
  Pallas kernels: 15.7 us -> 18.4 us
  other arithmetic: 2.07 us -> 3.71 us
    all_to_all x0 -> x1, blocking collectives: none -> 21.2 us  [exchange(): return lax.all_to_all(value, axis, 0, 0, tiled=True)]
    all_to_all x4 -> x3, waiting for transfers between devices: 33.8 us -> 18.9 us  [exchange(): return lax.all_to_all(value, axis, 0, 0, tiled=True)]
    ppermute x21 -> x26, waiting for transfers between devices: 31.4 us -> 45.5 us  [xor_swap(): return lax.ppermute(value, axis, [(i, i ^ bit) for i in range(size)])]
    slice x6 -> x1, local copies, waits for them, and re-layouts: 7.95 us -> 0.02 us  [spread_basis(): one[:, h:]]
    all_to_all x4 -> x3, starting transfers between devices: 17.9 us -> 10.4 us  [exchange(): return lax.all_to_all(value, axis, 0, 0, tiled=True)]
    unnamed x20 -> x16, local copies, waits for them, and re-layouts: 4.23 us -> 0.04 us
    ppermute x21 -> x26, starting transfers between devices: 29.4 us -> 31.8 us  [xor_swap(): return lax.ppermute(value, axis, [(i, i ^ bit) for i in range(size)])]
    broadcast_in_dim x0 -> x2, other arithmetic: none -> 2.1 us  [the longest x1 1.1 us: spread_basis(): one = xor_swap(rows(first, count)[None], 'fs', 1)]
  transfers between devices with their start and end apart: 25 -> 29, of which waited for: 15 -> 16; matrix products, arithmetic and copies ran while one was open for 8% -> 4% of each run, Pallas kernels for 3% -> 2%
where the time goes in v2:
time: 154 us
  waiting for transfers between devices  64.4 us (42%)
  starting transfers between devices  42.2 us (27%)
  blocking collectives  21.2 us (14%)
  Pallas kernels  18.4 us (12%)
  other arithmetic  3.71 us (2%)
  local copies, waits for them, and re-layouts  2.98 us (2%)
    ppermute x26, waiting for transfers between devices, xor_swap(): return lax.ppermute(value, axis, [(i, i ^ bit) for i in range(size)])  45.5 us
    ppermute x26, starting transfers between devices, xor_swap(): return lax.ppermute(value, axis, [(i, i ^ bit) for i in range(size)])  31.8 us
    all_to_all x1, blocking collectives, exchange(): return lax.all_to_all(value, axis, 0, 0, tiled=True)  21.2 us
    all_to_all x3, waiting for transfers between devices, exchange(): return lax.all_to_all(value, axis, 0, 0, tiled=True)  18.9 us
    all_to_all x3, starting transfers between devices, exchange(): return lax.all_to_all(value, axis, 0, 0, tiled=True)  10.4 us
    pallas_call x1, Pallas kernels, finish(): pl.pallas_call(functools.partial(finish_kernel, plan, n_tp), in_specs=[sm...  8.85 us
    pallas_call x1, Pallas kernels, tokens(): pl.pallas_call(functools.partial(token_kernel, tuple(((tuple(rel), first)...  3.36 us
  transfers between devices with their start and end apart: 29, of which 16 were waited for; matrix products, arithmetic and copies ran while one was open for 4% of the time, Pallas kernels for 2%

profile of v2, /device:TPU:0, one launch (start us, length us, event | category | flops | bytes accessed | tf_op | source)
XLA Modules:
  0.0 153.7 jit_solution(2037917207331886490)
XLA Ops:
  1.8 3.1 %collective-permute-start = (bf16[1,256,512]{2,1,0:T(8,128)(2,1)S(1)}, bf16[1,256,512]{2,1,0:T(8,128)(2,1)S(1)}, u32[]{:S(2)}, u32[]{:S(2)}) collective-permute-start(bf16[1,256,512]{2,1,0:T(8,128)(2,1)S(1)} %select_bitcast_fusion), channel_id=1, source_target_pairs={{0,8},{8,0},{16,24},{24,16},{1,9},{9,1},{17,25},{25,17},{2,10},{10... | collective-permute-start | bytes 786440 | tf_op jit(solution)/shard_map/ppermute | solution.py:31
  5.9 2.7 %collective-permute-start.3 = (bf16[1,128,512]{2,1,0:T(8,128)(2,1)S(1)}, bf16[1,128,512]{2,1,0:T(8,128)(2,1)S(1)}, u32[]{:S(2)}, u32[]{:S(2)}) collective-permute-start(bf16[1,128,512]{2,1,0:T(8,128)(2,1)S(1)} %select_bitcast_fusion.1), channel_id=1, source_target_pairs={{0,16},{8,24},{16,0},{24,8},{1,17},{9,25},{17,1},{25,9},{2,18},{10... | collective-permute-start | bytes 393224 | tf_op jit(solution)/shard_map/ppermute | solution.py:31
  8.6 4.7 %collective-permute-done.3.refs_3_ = bf16[1,128,512]{2,1,0:T(8,128)(2,1)S(1)} collective-permute-done((bf16[1,128,512]{2,1,0:T(8,128)(2,1)S(1)}, bf16[1,128,512]{2,1,0:T(8,128)(2,1)S(1)}, u32[]{:S(2)}, u32[]{:S(2)}) %collective-permute-start.3) | collective-permute-done | bytes 131104 | tf_op jit(solution)/shard_map/ppermute | solution.py:31
  13.2 3.5 %collective-permute-start.7 = (bf16[1,128,512]{2,1,0:T(8,128)(2,1)S(1)}, bf16[1,128,512]{2,1,0:T(8,128)(2,1)S(1)}, u32[]{:S(2)}, u32[]{:S(2)}) collective-permute-start(bf16[1,128,512]{2,1,0:T(8,128)(2,1)S(1)} %collective-permute-done.3.refs_3_), channel_id=1, source_target_pairs={{0,8},{8,0},{16,24},{24,16},{1,9},{9,1},{17,25},{25,17},{2,10},{10... | collective-permute-start | bytes 393224 | tf_op jit(solution)/shard_map/ppermute | solution.py:31
  16.7 2.4 %collective-permute-start.6 = (bf16[1,128,512]{2,1,0:T(8,128)(2,1)S(1)}, bf16[1,128,512]{2,1,0:T(8,128)(2,1)S(1)}, u32[]{:S(2)}, u32[]{:S(2)}) collective-permute-start(bf16[1,128,512]{2,1,0:T(8,128)(2,1)S(1)} %collective-permute-done.3.refs_3_), channel_id=1, source_target_pairs={{0,6},{2,4},{4,2},{6,0},{1,7},{3,5},{5,3},{7,1},{8,14},{10,12},{12... | collective-permute-start | bytes 393224 | tf_op jit(solution)/shard_map/ppermute | solution.py:31
  20.3 1.6 %collective-permute-start.2 = (bf16[1,128,512]{2,1,0:T(8,128)(2,1)S(1)}, bf16[1,128,512]{2,1,0:T(8,128)(2,1)S(1)}, u32[]{:S(2)}, u32[]{:S(2)}) collective-permute-start(bf16[1,128,512]{2,1,0:T(8,128)(2,1)S(1)} %get-tuple-element.42), channel_id=1, source_target_pairs={{0,4},{2,6},{4,0},{6,2},{1,5},{3,7},{5,1},{7,3},{8,12},{10,14},{12... | collective-permute-start | bytes 393224 | tf_op jit(solution)/shard_map/ppermute | solution.py:31
  23.8 1.8 %collective-permute-start.9 = (bf16[1,128,512]{2,1,0:T(8,128)(2,1)S(1)}, bf16[1,128,512]{2,1,0:T(8,128)(2,1)S(1)}, u32[]{:S(2)}, u32[]{:S(2)}) collective-permute-start(bf16[1,128,512]{2,1,0:T(8,128)(2,1)S(1)} %collective-permute-done.7.refs_7_), channel_id=1, source_target_pairs={{0,4},{2,6},{4,0},{6,2},{1,5},{3,7},{5,1},{7,3},{8,12},{10,14},{12... | collective-permute-start | bytes 393224 | tf_op jit(solution)/shard_map/ppermute | solution.py:31
  25.6 3.3 %collective-permute-done.5.refs_5_ = bf16[1,128,512]{2,1,0:T(8,128)(2,1)S(1)} collective-permute-done((bf16[1,128,512]{2,1,0:T(8,128)(2,1)S(1)}, bf16[1,128,512]{2,1,0:T(8,128)(2,1)S(1)}, u32[]{:S(2)}, u32[]{:S(2)}) %collective-permute-start.5) | collective-permute-done | bytes 131104 | tf_op jit(solution)/shard_map/ppermute | solution.py:31
  30.9 2.0 %collective-permute-done.9.refs_9_ = bf16[1,128,512]{2,1,0:T(8,128)(2,1)S(1)} collective-permute-done((bf16[1,128,512]{2,1,0:T(8,128)(2,1)S(1)}, bf16[1,128,512]{2,1,0:T(8,128)(2,1)S(1)}, u32[]{:S(2)}, u32[]{:S(2)}) %collective-permute-start.9) | collective-permute-done | bytes 131104 | tf_op jit(solution)/shard_map/ppermute | solution.py:31
  35.3 3.4 %tokens.1 = (bf16[2048,512]{1,0:T(8,128)(2,1)}, bf16[256,512]{1,0:T(8,128)(2,1)S(1)}) custom-call(s32[1]{0:T(128)} %bitcast.z_ref, s32[1]{0:T(128)} %bitcast.1.r_ref, s32[1]{0:T(128)} %bitcast.2.t_ref, bf16[256,2048]{1,0:T(8,128)(2,1)} %x_ref.1, bf16[512,512]{1,0:T(8,128)(2,1)} %own_q_ref.1, bf16[512,512]{1,0:T(8,128)(2,1)} %own_k_ref.1, ...), custom_call_target="tpu_custom_call" | custom-call | tf_op jit(solution)/shard_map/tokens/pallas_call | solution.py:148
  38.7 1.5 collective-permute-done.11.other_ref
  40.3 1.6 %terms.1 = bf16[4,4,32,1280]{3,2,1,0:T(8,128)(2,1)} custom-call(s32[1]{0:T(128)} %bitcast.2.t_ref, bf16[256,512]{1,0:T(8,128)(2,1)S(1)} %get-tuple-element.23.mine_ref, bf16[256,512]{1,0:T(8,128)(2,1)S(1)} %collective-permute-done.11.other_ref, bf16[256,1024]{1,0:T(8,128)(2,1)S(1)} %copy-done.1, bf16[256,256]{1,0:T(8,128)(2,1)S(1)} %copy-done.3), custom_call_target="tpu_custom_call" | custom-call | tf_op jit(solution)/shard_map/terms/pallas_call | solution.py:184
  41.9 21.2 %all_to_all.20.in_ref = bf16[4,4,32,1280]{3,2,1,0:T(8,128)(2,1)S(1)} all-to-all(bf16[4,4,32,1280]{3,2,1,0:T(8,128)(2,1)} %terms.1), channel_id=1, replica_groups=mesh['fs'=4,'rep'=4,'tp'=2] {'rep'}, dimensions={0} | all-to-all | bytes 2621440 | tf_op jit(solution)/shard_map/all_to_all | solution.py:35
  63.9 3.5 %all-to-all-start.1 = ((bf16[4,32,1280]{2,1,0:T(8,128)(2,1)}), bf16[4,32,1280]{2,1,0:T(8,128)(2,1)S(1)}, u32[]{:S(2)}, u32[]{:S(2)}) async-start(bf16[4,32,1280]{2,1,0:T(8,128)(2,1)} %sum_first.1), calls=%async_computation.1 | async-start | bytes 655360 | tf_op jit(solution)/shard_map/all_to_all | solution.py:35
  67.5 9.5 %all-to-all-done.1.got_ref = bf16[4,32,1280]{2,1,0:T(8,128)(2,1)S(1)} async-done(((bf16[4,32,1280]{2,1,0:T(8,128)(2,1)}), bf16[4,32,1280]{2,1,0:T(8,128)(2,1)S(1)}, u32[]{:S(2)}, u32[]{:S(2)}) %all-to-all-start.1) | async-done | bytes 327712 | tf_op jit(solution)/shard_map/all_to_all | solution.py:35
  77.9 3.5 %all-to-all-start.2 = ((bf16[4,32,1280]{2,1,0:T(8,128)(2,1)}), bf16[4,32,1280]{2,1,0:T(8,128)(2,1)S(1)}, u32[]{:S(2)}, u32[]{:S(2)}) async-start(bf16[4,32,1280]{2,1,0:T(8,128)(2,1)} %get-tuple-element.24), calls=%async_computation.2 | async-start | bytes 655360 | tf_op jit(solution)/shard_map/all_to_all | solution.py:35
  81.3 1.6 %dynamic-slice_convert_fusion.2 = (bf16[128,256]{1,0:T(8,128)(2,1)}, bf16[128,256]{1,0:T(8,128)(2,1)S(1)}) fusion(f32[512,256]{1,0:T(8,128)} %wk_ref.1, s32[]{:T(128)S(6)} %select_n.41, s32[]{:T(128)S(6)} %select_n.35), kind=kLoop, calls=%fused_computation.5 | loop fusion | bytes 262152 | tf_op jit(solution)/shard_map/convert_element_type | solution.py:510
  85.0 2.9 %collective-permute-start.16 = (bf16[1,128,1280]{2,1,0:T(8,128)(2,1)}, bf16[1,128,1280]{2,1,0:T(8,128)(2,1)S(1)}, u32[]{:S(2)}, u32[]{:S(2)}) collective-permute-start(bf16[1,128,1280]{2,1,0:T(8,128)(2,1)} %maximum_bitcast_fusion), channel_id=1, source_target_pairs={{0,16},{8,24},{16,0},{24,8},{1,17},{9,25},{17,1},{25,9},{2,18},{10... | collective-permute-start | bytes 983048 | tf_op jit(solution)/shard_map/ppermute | solution.py:31
  89.3 9.4 %all-to-all-done.2.got_ref = bf16[4,32,1280]{2,1,0:T(8,128)(2,1)S(1)} async-done(((bf16[4,32,1280]{2,1,0:T(8,128)(2,1)}), bf16[4,32,1280]{2,1,0:T(8,128)(2,1)S(1)}, u32[]{:S(2)}, u32[]{:S(2)}) %all-to-all-start.2) | async-done | bytes 327712 | tf_op jit(solution)/shard_map/all_to_all | solution.py:35
  99.9 3.5 %all-to-all-start.3 = ((bf16[4,4,32,1280]{3,2,1,0:T(8,128)(2,1)}), bf16[4,4,32,1280]{3,2,1,0:T(8,128)(2,1)S(1)}, u32[]{:S(2)}, u32[]{:S(2)}) async-start(bf16[4,4,32,1280]{3,2,1,0:T(8,128)(2,1)} %plane.1), calls=%async_computation.3 | async-start | bytes 2621440 | tf_op jit(solution)/shard_map/all_to_all | solution.py:35
  105.2 7.1 %collective-permute-done.16.refs_2_ = bf16[1,128,1280]{2,1,0:T(8,128)(2,1)S(1)} collective-permute-done((bf16[1,128,1280]{2,1,0:T(8,128)(2,1)}, bf16[1,128,1280]{2,1,0:T(8,128)(2,1)S(1)}, u32[]{:S(2)}, u32[]{:S(2)}) %collective-permute-start.16) | collective-permute-done | bytes 327712 | tf_op jit(solution)/shard_map/ppermute | solution.py:31
  112.9 5.5 %collective-permute-done.22.refs_8_ = bf16[1,128,1280]{2,1,0:T(8,128)(2,1)} collective-permute-done((bf16[1,128,1280]{2,1,0:T(8,128)(2,1)S(1)}, bf16[1,128,1280]{2,1,0:T(8,128)(2,1)}, u32[]{:S(2)}, u32[]{:S(2)}) %collective-permute-start.22) | collective-permute-done | bytes 327712 | tf_op jit(solution)/shard_map/ppermute | solution.py:31
  119.6 1.6 %collective-permute-done.20.refs_6_ = bf16[1,128,1280]{2,1,0:T(8,128)(2,1)} collective-permute-done((bf16[1,128,1280]{2,1,0:T(8,128)(2,1)S(1)}, bf16[1,128,1280]{2,1,0:T(8,128)(2,1)}, u32[]{:S(2)}, u32[]{:S(2)}) %collective-permute-start.20) | collective-permute-done | bytes 327712 | tf_op jit(solution)/shard_map/ppermute | solution.py:31
  121.2 6.8 %collective-permute-done.18.refs_4_ = bf16[1,128,1280]{2,1,0:T(8,128)(2,1)} collective-permute-done((bf16[1,128,1280]{2,1,0:T(8,128)(2,1)S(1)}, bf16[1,128,1280]{2,1,0:T(8,128)(2,1)}, u32[]{:S(2)}, u32[]{:S(2)}) %collective-permute-start.18) | collective-permute-done | bytes 327712 | tf_op jit(solution)/shard_map/ppermute | solution.py:31
  128.0 1.5 collective-permute-start.23
  130.0 1.5 collective-permute-start.19
  131.5 1.5 collective-permute-start.25
  133.0 1.6 %directions.1 = (f32[2,128,1024]{2,1,0:T(8,128)}, f32[2,128,256]{2,1,0:T(8,128)}, bf16[512,1024]{1,0:T(8,128)(2,1)S(1)}, bf16[512,256]{1,0:T(8,128)(2,1)S(1)}, f32[16,128]{1,0:T(8,128)S(1)}) custom-call(s32[1]{0:T(128)} %bitcast.z_ref, bf16[4,4,32,1280]{3,2,1,0:T(8,128)(2,1)S(1)} %all-to-all-done.3.got_ref, f32[2,128,1024]{2,1,0:T(8,128)S(1)} %copy-done, ...), custom_call_target="tpu_custom_call" | custom-call | tf_op jit(solution)/shard_map/directions/pallas_call | solution.py:303
  134.6 3.2 %collective-permute-done.23.refs_9_ = bf16[1,128,1280]{2,1,0:T(8,128)(2,1)} collective-permute-done((bf16[1,128,1280]{2,1,0:T(8,128)(2,1)}, bf16[1,128,1280]{2,1,0:T(8,128)(2,1)}, u32[]{:S(2)}, u32[]{:S(2)}) %collective-permute-start.23) | collective-permute-done | bytes 327712 | tf_op jit(solution)/shard_map/ppermute | solution.py:31
  137.8 3.5 %collective-permute-done.21.refs_7_ = bf16[1,128,1280]{2,1,0:T(8,128)(2,1)} collective-permute-done((bf16[1,128,1280]{2,1,0:T(8,128)(2,1)}, bf16[1,128,1280]{2,1,0:T(8,128)(2,1)}, u32[]{:S(2)}, u32[]{:S(2)}) %collective-permute-start.21) | collective-permute-done | bytes 327712 | tf_op jit(solution)/shard_map/ppermute | solution.py:31
  141.3 3.5 %collective-permute-done.25.refs_11_ = bf16[1,128,1280]{2,1,0:T(8,128)(2,1)} collective-permute-done((bf16[1,128,1280]{2,1,0:T(8,128)(2,1)}, bf16[1,128,1280]{2,1,0:T(8,128)(2,1)}, u32[]{:S(2)}, u32[]{:S(2)}) %collective-permute-start.25) | collective-permute-done | bytes 327712 | tf_op jit(solution)/shard_map/ppermute | solution.py:31
  144.8 8.9 %finish.1 = (f32[512,1024]{1,0:T(8,128)}, f32[512,256]{1,0:T(8,128)}, f32[512,1024]{1,0:T(8,128)}, f32[512,256]{1,0:T(8,128)}, bf16[2048,1024]{1,0:T(8,128)(2,1)}, /*index=5*/bf16[2048,256]{1,0:T(8,128)(2,1)}) custom-call(s32[1]{0:T(128)} %bitcast.z_ref, s32[1]{0:T(128)} %bitcast.1.r_ref, s32[1]{0:T(128)} %bitcast.2.t_ref, ...), custom_call_target="tpu_custom_call" | custom-call | tf_op jit(solution)/shard_map/finish/pallas_call | solution.py:463
  (59 shorter events, 20.3 us)
Async XLA Ops:
  1.8 18.5 %collective-permute-start = (bf16[1,256,512]{2,1,0:T(8,128)(2,1)S(1)}, bf16[1,256,512]{2,1,0:T(8,128)(2,1)S(1)}, u32[]{:S(2)}, u32[]{:S(2)}) collective-permute-start(bf16[1,256,512]{2,1,0:T(8,128)(2,1)S(1)} %select_bitcast_fusion), channel_id=1, source_target_pairs={{0,8},{8,0},{16,24},{24,16},{1,9},{9,1},{17,25},{25,17},{2,10},{10... | collective-permute-start | bytes 786440 | tf_op jit(solution)/shard_map/ppermute | solution.py:31
  5.9 34.4 %copy-start.1 = (bf16[256,1024]{1,0:T(8,128)(2,1)S(1)}, bf16[256,1024]{1,0:T(8,128)(2,1)}, u32[]{:S(2)}) copy-start(bf16[256,1024]{1,0:T(8,128)(2,1)} %cq_ref.1) | copy-start | bytes 1572868
  5.9 34.4 %copy-start.3 = (bf16[256,256]{1,0:T(8,128)(2,1)S(1)}, bf16[256,256]{1,0:T(8,128)(2,1)}, u32[]{:S(2)}) copy-start(bf16[256,256]{1,0:T(8,128)(2,1)} %ck_ref.1) | copy-start | bytes 393220
  5.9 7.3 %collective-permute-start.3 = (bf16[1,128,512]{2,1,0:T(8,128)(2,1)S(1)}, bf16[1,128,512]{2,1,0:T(8,128)(2,1)S(1)}, u32[]{:S(2)}, u32[]{:S(2)}) collective-permute-start(bf16[1,128,512]{2,1,0:T(8,128)(2,1)S(1)} %select_bitcast_fusion.1), channel_id=1, source_target_pairs={{0,16},{8,24},{16,0},{24,8},{1,17},{9,25},{17,1},{25,9},{2,18},{10... | collective-permute-start | bytes 393224 | tf_op jit(solution)/shard_map/ppermute | solution.py:31
  13.2 8.6 %collective-permute-start.7 = (bf16[1,128,512]{2,1,0:T(8,128)(2,1)S(1)}, bf16[1,128,512]{2,1,0:T(8,128)(2,1)S(1)}, u32[]{:S(2)}, u32[]{:S(2)}) collective-permute-start(bf16[1,128,512]{2,1,0:T(8,128)(2,1)S(1)} %collective-permute-done.3.refs_3_), channel_id=1, source_target_pairs={{0,8},{8,0},{16,24},{24,16},{1,9},{9,1},{17,25},{25,17},{2,10},{10... | collective-permute-start | bytes 393224 | tf_op jit(solution)/shard_map/ppermute | solution.py:31
  16.7 7.1 %collective-permute-start.6 = (bf16[1,128,512]{2,1,0:T(8,128)(2,1)S(1)}, bf16[1,128,512]{2,1,0:T(8,128)(2,1)S(1)}, u32[]{:S(2)}, u32[]{:S(2)}) collective-permute-start(bf16[1,128,512]{2,1,0:T(8,128)(2,1)S(1)} %collective-permute-done.3.refs_3_), channel_id=1, source_target_pairs={{0,6},{2,4},{4,2},{6,0},{1,7},{3,5},{5,3},{7,1},{8,14},{10,12},{12... | collective-permute-start | bytes 393224 | tf_op jit(solution)/shard_map/ppermute | solution.py:31
  19.2 9.7 %collective-permute-start.5 = (bf16[1,128,512]{2,1,0:T(8,128)(2,1)S(1)}, bf16[1,128,512]{2,1,0:T(8,128)(2,1)S(1)}, u32[]{:S(2)}, u32[]{:S(2)}) collective-permute-start(bf16[1,128,512]{2,1,0:T(8,128)(2,1)S(1)} %collective-permute-done.3.refs_3_), channel_id=1, source_target_pairs={{0,4},{2,6},{4,0},{6,2},{1,5},{3,7},{5,1},{7,3},{8,12},{10,14},{12... | collective-permute-start | bytes 393224 | tf_op jit(solution)/shard_map/ppermute | solution.py:31
  19.7 10.3 %collective-permute-start.4 = (bf16[1,128,512]{2,1,0:T(8,128)(2,1)S(1)}, bf16[1,128,512]{2,1,0:T(8,128)(2,1)S(1)}, u32[]{:S(2)}, u32[]{:S(2)}) collective-permute-start(bf16[1,128,512]{2,1,0:T(8,128)(2,1)S(1)} %collective-permute-done.3.refs_3_), channel_id=1, source_target_pairs={{0,2},{2,0},{4,6},{6,4},{1,3},{3,1},{5,7},{7,5},{8,10},{10,8},{12,... | collective-permute-start | bytes 393224 | tf_op jit(solution)/shard_map/ppermute | solution.py:31
  20.3 13.6 %collective-permute-start.2 = (bf16[1,128,512]{2,1,0:T(8,128)(2,1)S(1)}, bf16[1,128,512]{2,1,0:T(8,128)(2,1)S(1)}, u32[]{:S(2)}, u32[]{:S(2)}) collective-permute-start(bf16[1,128,512]{2,1,0:T(8,128)(2,1)S(1)} %get-tuple-element.42), channel_id=1, source_target_pairs={{0,4},{2,6},{4,0},{6,2},{1,5},{3,7},{5,1},{7,3},{8,12},{10,14},{12... | collective-permute-start | bytes 393224 | tf_op jit(solution)/shard_map/ppermute | solution.py:31
  21.8 9.1 %collective-permute-start.10 = (bf16[1,128,512]{2,1,0:T(8,128)(2,1)S(1)}, bf16[1,128,512]{2,1,0:T(8,128)(2,1)S(1)}, u32[]{:S(2)}, u32[]{:S(2)}) collective-permute-start(bf16[1,128,512]{2,1,0:T(8,128)(2,1)S(1)} %collective-permute-done.7.refs_7_), channel_id=1, source_target_pairs={{0,6},{2,4},{4,2},{6,0},{1,7},{3,5},{5,3},{7,1},{8,14},{10,12},{12... | collective-permute-start | bytes 393224 | tf_op jit(solution)/shard_map/ppermute | solution.py:31
  23.8 9.1 %collective-permute-start.9 = (bf16[1,128,512]{2,1,0:T(8,128)(2,1)S(1)}, bf16[1,128,512]{2,1,0:T(8,128)(2,1)S(1)}, u32[]{:S(2)}, u32[]{:S(2)}) collective-permute-start(bf16[1,128,512]{2,1,0:T(8,128)(2,1)S(1)} %collective-permute-done.7.refs_7_), channel_id=1, source_target_pairs={{0,4},{2,6},{4,0},{6,2},{1,5},{3,7},{5,1},{7,3},{8,12},{10,14},{12... | collective-permute-start | bytes 393224 | tf_op jit(solution)/shard_map/ppermute | solution.py:31
  28.9 5.0 %collective-permute-start.8 = (bf16[1,128,512]{2,1,0:T(8,128)(2,1)S(1)}, bf16[1,128,512]{2,1,0:T(8,128)(2,1)S(1)}, u32[]{:S(2)}, u32[]{:S(2)}) collective-permute-start(bf16[1,128,512]{2,1,0:T(8,128)(2,1)S(1)} %collective-permute-done.7.refs_7_), channel_id=1, source_target_pairs={{0,2},{2,0},{4,6},{6,4},{1,3},{3,1},{5,7},{7,5},{8,10},{10,8},{12,... | collective-permute-start | bytes 393224 | tf_op jit(solution)/shard_map/ppermute | solution.py:31
  30.0 5.3 %collective-permute-start.1 = (bf16[1,128,512]{2,1,0:T(8,128)(2,1)S(1)}, bf16[1,128,512]{2,1,0:T(8,128)(2,1)S(1)}, u32[]{:S(2)}, u32[]{:S(2)}) collective-permute-start(bf16[1,128,512]{2,1,0:T(8,128)(2,1)S(1)} %get-tuple-element.43), channel_id=1, source_target_pairs={{0,2},{2,0},{4,6},{6,4},{1,3},{3,1},{5,7},{7,5},{8,10},{10,8},{12,... | collective-permute-start | bytes 393224 | tf_op jit(solution)/shard_map/ppermute | solution.py:31
  38.6 1.6 %collective-permute-start.11 = (bf16[256,512]{1,0:T(8,128)(2,1)S(1)}, bf16[256,512]{1,0:T(8,128)(2,1)S(1)}, u32[]{:S(2)}, u32[]{:S(2)}) collective-permute-start(bf16[256,512]{1,0:T(8,128)(2,1)S(1)} %get-tuple-element.23.mine_ref), channel_id=1, source_target_pairs={{0,1},{1,0},{2,3},{3,2},{4,5},{5,4},{6,7},{7,6},{8,9},{9,8},{10,11... | collective-permute-start | bytes 786440 | tf_op jit(solution)/shard_map/ppermute | solution.py:31
  63.9 13.1 %all-to-all-start.1 = ((bf16[4,32,1280]{2,1,0:T(8,128)(2,1)}), bf16[4,32,1280]{2,1,0:T(8,128)(2,1)S(1)}, u32[]{:S(2)}, u32[]{:S(2)}) async-start(bf16[4,32,1280]{2,1,0:T(8,128)(2,1)} %sum_first.1), calls=%async_computation.1 | async-start | bytes 655360 | tf_op jit(solution)/shard_map/all_to_all | solution.py:35
  67.4 77.4 %collective-permute-start.13 = (bf16[2048,512]{1,0:T(8,128)(2,1)}, bf16[2048,512]{1,0:T(8,128)(2,1)}, u32[]{:S(2)}, u32[]{:S(2)}) collective-permute-start(bf16[2048,512]{1,0:T(8,128)(2,1)} %get-tuple-element.29.mine_ref), channel_id=1, source_target_pairs={{0,1},{1,0},{2,3},{3,2},{4,5},{5,4},{6,7},{7,6},{8,9},{9,8},{10,11... | collective-permute-start | bytes 6291464 | tf_op jit(solution)/shard_map/ppermute | solution.py:31
  77.9 20.9 %all-to-all-start.2 = ((bf16[4,32,1280]{2,1,0:T(8,128)(2,1)}), bf16[4,32,1280]{2,1,0:T(8,128)(2,1)S(1)}, u32[]{:S(2)}, u32[]{:S(2)}) async-start(bf16[4,32,1280]{2,1,0:T(8,128)(2,1)} %get-tuple-element.24), calls=%async_computation.2 | async-start | bytes 655360 | tf_op jit(solution)/shard_map/all_to_all | solution.py:35
  85.0 27.3 %collective-permute-start.16 = (bf16[1,128,1280]{2,1,0:T(8,128)(2,1)}, bf16[1,128,1280]{2,1,0:T(8,128)(2,1)S(1)}, u32[]{:S(2)}, u32[]{:S(2)}) collective-permute-start(bf16[1,128,1280]{2,1,0:T(8,128)(2,1)} %maximum_bitcast_fusion), channel_id=1, source_target_pairs={{0,16},{8,24},{16,0},{24,8},{1,17},{9,25},{17,1},{25,9},{2,18},{10... | collective-permute-start | bytes 983048 | tf_op jit(solution)/shard_map/ppermute | solution.py:31
  87.9 24.4 %collective-permute-start.14 = (bf16[1,128,1280]{2,1,0:T(8,128)(2,1)}, bf16[1,128,1280]{2,1,0:T(8,128)(2,1)S(1)}, u32[]{:S(2)}, u32[]{:S(2)}) collective-permute-start(bf16[1,128,1280]{2,1,0:T(8,128)(2,1)} %maximum_bitcast_fusion), channel_id=1, source_target_pairs={{0,8},{8,0},{16,24},{24,16},{1,9},{9,1},{17,25},{25,17},{2,10},{10... | collective-permute-start | bytes 983048 | tf_op jit(solution)/shard_map/ppermute | solution.py:31
  99.9 33.1 %all-to-all-start.3 = ((bf16[4,4,32,1280]{3,2,1,0:T(8,128)(2,1)}), bf16[4,4,32,1280]{3,2,1,0:T(8,128)(2,1)S(1)}, u32[]{:S(2)}, u32[]{:S(2)}) async-start(bf16[4,4,32,1280]{3,2,1,0:T(8,128)(2,1)} %plane.1), calls=%async_computation.3 | async-start | bytes 2621440 | tf_op jit(solution)/shard_map/all_to_all | solution.py:35
  104.4 14.0 %collective-permute-start.22 = (bf16[1,128,1280]{2,1,0:T(8,128)(2,1)S(1)}, bf16[1,128,1280]{2,1,0:T(8,128)(2,1)}, u32[]{:S(2)}, u32[]{:S(2)}) collective-permute-start(bf16[1,128,1280]{2,1,0:T(8,128)(2,1)S(1)} %maximum_bitcast_fusion.1), channel_id=1, source_target_pairs={{0,16},{8,24},{16,0},{24,8},{1,17},{9,25},{17,1},{25,9},{2,18},{10... | collective-permute-start | bytes 983048 | tf_op jit(solution)/shard_map/ppermute | solution.py:31
  104.4 16.8 %collective-permute-start.20 = (bf16[1,128,1280]{2,1,0:T(8,128)(2,1)S(1)}, bf16[1,128,1280]{2,1,0:T(8,128)(2,1)}, u32[]{:S(2)}, u32[]{:S(2)}) collective-permute-start(bf16[1,128,1280]{2,1,0:T(8,128)(2,1)S(1)} %maximum_bitcast_fusion.1), channel_id=1, source_target_pairs={{0,8},{8,0},{16,24},{24,16},{1,9},{9,1},{17,25},{25,17},{2,10},{10... | collective-permute-start | bytes 983048 | tf_op jit(solution)/shard_map/ppermute | solution.py:31
  112.3 32.6 %copy-start.4 = (bf16[1,128,1280]{2,1,0:T(8,128)(2,1)}, bf16[1,128,1280]{2,1,0:T(8,128)(2,1)S(1)}, u32[]{:S(2)}) copy-start(bf16[1,128,1280]{2,1,0:T(8,128)(2,1)S(1)} %collective-permute-done.16.refs_2_) | copy-start | bytes 983044
  112.3 15.7 %collective-permute-start.18 = (bf16[1,128,1280]{2,1,0:T(8,128)(2,1)S(1)}, bf16[1,128,1280]{2,1,0:T(8,128)(2,1)}, u32[]{:S(2)}, u32[]{:S(2)}) collective-permute-start(bf16[1,128,1280]{2,1,0:T(8,128)(2,1)S(1)} %collective-permute-done.16.refs_2_), channel_id=1, source_target_pairs={{0,8},{8,0},{16,24},{24,16},{1,9},{9,1},{17,25},{25,17},{2,10},{10... | collective-permute-start | bytes 983048 | tf_op jit(solution)/shard_map/ppermute | solution.py:31
  112.3 17.2 %collective-permute-start.17 = (bf16[1,128,1280]{2,1,0:T(8,128)(2,1)S(1)}, bf16[1,128,1280]{2,1,0:T(8,128)(2,1)S(1)}, u32[]{:S(2)}, u32[]{:S(2)}) collective-permute-start(bf16[1,128,1280]{2,1,0:T(8,128)(2,1)S(1)} %collective-permute-done.16.refs_2_), channel_id=1, source_target_pairs={{0,2},{2,0},{4,6},{6,4},{1,3},{3,1},{5,7},{7,5},{8,10},{10,8},{12,... | collective-permute-start | bytes 983048 | tf_op jit(solution)/shard_map/ppermute | solution.py:31
  118.3 11.7 %collective-permute-start.15 = (bf16[1,128,1280]{2,1,0:T(8,128)(2,1)S(1)}, bf16[1,128,1280]{2,1,0:T(8,128)(2,1)S(1)}, u32[]{:S(2)}, u32[]{:S(2)}) collective-permute-start(bf16[1,128,1280]{2,1,0:T(8,128)(2,1)S(1)} %collective-permute-done.14.refs_0_), channel_id=1, source_target_pairs={{0,2},{2,0},{4,6},{6,4},{1,3},{3,1},{5,7},{7,5},{8,10},{10,8},{12,... | collective-permute-start | bytes 983048 | tf_op jit(solution)/shard_map/ppermute | solution.py:31
  121.2 10.3 %collective-permute-start.24 = (bf16[1,128,1280]{2,1,0:T(8,128)(2,1)}, bf16[1,128,1280]{2,1,0:T(8,128)(2,1)}, u32[]{:S(2)}, u32[]{:S(2)}) collective-permute-start(bf16[1,128,1280]{2,1,0:T(8,128)(2,1)} %collective-permute-done.22.refs_8_), channel_id=1, source_target_pairs={{0,8},{8,0},{16,24},{24,16},{1,9},{9,1},{17,25},{25,17},{2,10},{10... | collective-permute-start | bytes 983048 | tf_op jit(solution)/shard_map/ppermute | solution.py:31
  128.0 9.8 %collective-permute-start.23 = (bf16[1,128,1280]{2,1,0:T(8,128)(2,1)}, bf16[1,128,1280]{2,1,0:T(8,128)(2,1)}, u32[]{:S(2)}, u32[]{:S(2)}) collective-permute-start(bf16[1,128,1280]{2,1,0:T(8,128)(2,1)} %collective-permute-done.22.refs_8_), channel_id=1, source_target_pairs={{0,4},{2,6},{4,0},{6,2},{1,5},{3,7},{5,1},{7,3},{8,12},{10,14},{12... | collective-permute-start | bytes 983048 | tf_op jit(solution)/shard_map/ppermute | solution.py:31
  129.5 11.8 %collective-permute-start.21 = (bf16[1,128,1280]{2,1,0:T(8,128)(2,1)}, bf16[1,128,1280]{2,1,0:T(8,128)(2,1)}, u32[]{:S(2)}, u32[]{:S(2)}) collective-permute-start(bf16[1,128,1280]{2,1,0:T(8,128)(2,1)} %collective-permute-done.20.refs_6_), channel_id=1, source_target_pairs={{0,4},{2,6},{4,0},{6,2},{1,5},{3,7},{5,1},{7,3},{8,12},{10,14},{12... | collective-permute-start | bytes 983048 | tf_op jit(solution)/shard_map/ppermute | solution.py:31
  130.0 11.3 %collective-permute-start.19 = (bf16[1,128,1280]{2,1,0:T(8,128)(2,1)}, bf16[1,128,1280]{2,1,0:T(8,128)(2,1)}, u32[]{:S(2)}, u32[]{:S(2)}) collective-permute-start(bf16[1,128,1280]{2,1,0:T(8,128)(2,1)} %collective-permute-done.18.refs_4_), channel_id=1, source_target_pairs={{0,2},{2,0},{4,6},{6,4},{1,3},{3,1},{5,7},{7,5},{8,10},{10,8},{12,... | collective-permute-start | bytes 983048 | tf_op jit(solution)/shard_map/ppermute | solution.py:31
  131.5 13.3 %collective-permute-start.25 = (bf16[1,128,1280]{2,1,0:T(8,128)(2,1)}, bf16[1,128,1280]{2,1,0:T(8,128)(2,1)}, u32[]{:S(2)}, u32[]{:S(2)}) collective-permute-start(bf16[1,128,1280]{2,1,0:T(8,128)(2,1)} %collective-permute-done.24.refs_10_), channel_id=1, source_target_pairs={{0,4},{2,6},{4,0},{6,2},{1,5},{3,7},{5,1},{7,3},{8,12},{10,14},{12... | collective-permute-start | bytes 983048 | tf_op jit(solution)/shard_map/ppermute | solution.py:31
  137.8 7.0 %collective-permute-start.12 = (f32[16,128]{1,0:T(8,128)S(1)}, f32[16,128]{1,0:T(8,128)S(1)}, u32[]{:S(2)}, u32[]{:S(2)}) collective-permute-start(f32[16,128]{1,0:T(8,128)S(1)} %get-tuple-element.26.sums_ref), channel_id=1, source_target_pairs={{0,1},{1,0},{2,3},{3,2},{4,5},{5,4},{6,7},{7,6},{8,9},{9,8},{10,11... | collective-permute-start | bytes 24584 | tf_op jit(solution)/shard_map/ppermute | solution.py:31
  (5 other events, 87.3 us)

commit v3 on v2

--- a/solution.py
+++ b/solution.py
@@ -72,6 +72,11 @@
                 for i in range(1, n_r):
                     near = xor_swap(got, "rep", i)
                     pieces.append((rels, near, lambda r, i=i: jnp.bitwise_xor(r, i), n))
+            elif len(own) == 2 and m == 1 and len(rels) == 1 and n == 2 and got.shape[1] % 32 == 0:
+                h = got.shape[1] // 2
+                for i, half in enumerate((got[:, :h], got[:, h:])):
+                    near = xor_swap(half, "rep", 1 + i)
+                    pieces.append((rels, near, lambda r, i=i: (3 - 2 * parity(r), i), n))
             elif len(own) == 2:
                 near = xor_swap(got, "rep", 1 + m)
                 pieces.append((rels, near, lambda r, m=m: 2 + m - 2 * parity(r), n))
@@ -111,7 +116,8 @@
 
 def token_kernel(rels, z_ref, r_ref, t_ref, x_ref, own_q_ref, own_k_ref, *refs):
     parts, (basis_ref, token_ref) = refs[: len(rels)], refs[len(rels) : len(rels) + 2]
-    x_vmem, basis_vmem, x_sem, own_sem, sems, out_sem = refs[len(rels) + 2 :]
+    x_vmem, x_sem, own_sem, sems = refs[len(rels) + 2 :]
+    basis_vmem = basis_ref
     x_load = pltpu.make_async_copy(x_ref, x_vmem, x_sem)
     x_load.start()
     z = z_ref[0]
@@ -134,10 +140,7 @@
     pltpu.make_async_copy(own_q_ref, basis_vmem.at[own_at], own_sem).wait()
     for load in loads:
         load.wait()
-    store = pltpu.make_async_copy(basis_vmem, basis_ref, out_sem)
-    store.start()
     token_ref[...] = jnp.dot(x_vmem[...], basis_vmem[...], preferred_element_type=F32).astype(BF)
-    store.wait()
 
 
 def tokens(z, r, t, x, own_q, own_k, parts):
@@ -148,16 +151,13 @@
     return pl.pallas_call(
         functools.partial(token_kernel, tuple((tuple(rel), first) for rel, _, first, _ in parts)),
         in_specs=[pl.BlockSpec(memory_space=pltpu.SMEM)] * 3 + [hbm] * len(sources),
-        out_specs=[hbm, whole(token)],
-        grid=(1,),
-        out_shape=[pltpu.HBM(shape, BF), pltpu.VMEM(token, BF)],
+        out_specs=[pl.BlockSpec(memory_space=pltpu.VMEM)] * 2,
+        out_shape=[pltpu.VMEM(shape, BF), pltpu.VMEM(token, BF)],
         scratch_shapes=[
             pltpu.VMEM(x.shape, BF),
-            pltpu.VMEM(shape, BF),
             pltpu.SemaphoreType.DMA,
             pltpu.SemaphoreType.DMA,
             pltpu.SemaphoreType.DMA((len(parts), max(len(rel) for rel, _, _, _ in parts))),
-            pltpu.SemaphoreType.DMA,
         ],
         compiler_params=SMALL,
         name="tokens",
@@ -329,7 +329,9 @@
     for i, (rels, first) in enumerate(plan):
         if rel in rels:
             j = rels.index(rel)
-            at = pl.ds(pl.multiple_of(first(r) * h, 16), pieces[i].shape[1])
+            at = first(r)
+            at = at[0] * h + at[1] * (h // 2) if isinstance(at, tuple) else at * h
+            at = pl.ds(pl.multiple_of(at, 16), pieces[i].shape[1])
             loads.append(
                 pltpu.make_async_copy(pieces[i].at[j], to.at[slots[rel], at], sems.at[i, j])
             )
@@ -370,7 +372,7 @@
     rank = dq_ref.shape[0]
     slots = slots_of(plan)
     order = [*slots]
-    order = [order[0], 0, *order[1:]]
+    order = [0, *order]
 
     def block(rel):
         return pl.ds(pl.multiple_of(jnp.bitwise_xor(z, rel) * rows, rows), rows)
@@ -456,9 +458,9 @@
         ((rows * n_f, cols_q), BF),
         ((rows * n_f, cols_k), BF),
     ]
-    inside = [in_space(a, pltpu.VMEM) for a in (sums, other_sums, dir_q, dir_k)]
+    inside = [in_space(a, pltpu.VMEM) for a in (sums, other_sums, dir_q, dir_k, mine)]
     outside = [
-        in_space(a, pltpu.HBM) for a in (mine, other, weight_q, weight_k, *[p[1] for p in pieces])
+        in_space(a, pltpu.HBM) for a in (other, weight_q, weight_k, *[p[1] for p in pieces])
     ]
     return pl.pallas_call(
         functools.partial(finish_kernel, plan, n_tp),

time: 154 us -> 164 us (1.065)
  blocking collectives: 21.2 us -> 0 us
  local copies, waits for them, and re-layouts: 2.98 us -> 17.2 us
  starting transfers between devices: 42.2 us -> 53.2 us
  waiting for transfers between devices: 64.4 us -> 71.2 us
  Pallas kernels: 18.4 us -> 16 us
    all_to_all x1 -> x0, blocking collectives: 21.2 us -> none  [exchange(): return lax.all_to_all(value, axis, 0, 0, tiled=True)]
    all_to_all x3 -> x4, waiting for transfers between devices: 18.9 us -> 37.1 us  [exchange(): return lax.all_to_all(value, axis, 0, 0, tiled=True)]
    unnamed x16 -> x38, local copies, waits for them, and re-layouts: 0.04 us -> 11.6 us
    ppermute x26 -> x27, waiting for transfers between devices: 45.5 us -> 34.1 us  [xor_swap(): return lax.ppermute(value, axis, [(i, i ^ bit) for i in range(size)])]
    ppermute x26 -> x27, starting transfers between devices: 31.8 us -> 39.1 us  [xor_swap(): return lax.ppermute(value, axis, [(i, i ^ bit) for i in range(size)])]
    all_to_all x3 -> x4, starting transfers between devices: 10.4 us -> 14.1 us  [exchange(): return lax.all_to_all(value, axis, 0, 0, tiled=True)]
    pallas_call x1, Pallas kernels: 8.85 us -> 7.1 us  [finish(): pl.pallas_call(functools.partial(finish_kernel, plan, n_tp), in_specs=[sm...]
  transfers between devices with their start and end apart: 29 -> 31, of which waited for: 16 -> 15; matrix products, arithmetic and copies ran while one was open for 4% -> 6% of each run, Pallas kernels for 2% -> 3%
where the time goes in v3:
time: 164 us; the launch traced here: 163 us
  waiting for transfers between devices  71.2 us (43%)
  starting transfers between devices  53.2 us (32%)
  local copies, waits for them, and re-layouts  17.2 us (10%)
  Pallas kernels  16 us (10%)
  other arithmetic  4.54 us (3%)
    ppermute x27, starting transfers between devices, xor_swap(): return lax.ppermute(value, axis, [(i, i ^ bit) for i in range(size)])  39.1 us
    all_to_all x4, waiting for transfers between devices, exchange(): return lax.all_to_all(value, axis, 0, 0, tiled=True)  37.1 us
    ppermute x27, waiting for transfers between devices, xor_swap(): return lax.ppermute(value, axis, [(i, i ^ bit) for i in range(size)])  34.1 us
    all_to_all x4, starting transfers between devices, exchange(): return lax.all_to_all(value, axis, 0, 0, tiled=True)  14.1 us
    unnamed x38, local copies, waits for them, and re-layouts  11.6 us
    pallas_call x1, Pallas kernels, finish(): pl.pallas_call(functools.partial(finish_kernel, plan, n_tp), in_specs=[sm...  7.1 us
  transfers between devices with their start and end apart: 31, of which 15 were waited for; matrix products, arithmetic and copies ran while one was open for 6% of the time, Pallas kernels for 3%

profile of v3, /device:TPU:0, one launch (start us, length us, event | category | flops | bytes accessed | tf_op | source)
XLA Modules:
  0.0 162.9 jit_solution(6501217062957445632)
XLA Ops:
  1.8 3.1 %collective-permute-start = (bf16[1,256,512]{2,1,0:T(8,128)(2,1)S(1)}, bf16[1,256,512]{2,1,0:T(8,128)(2,1)S(1)}, u32[]{:S(2)}, u32[]{:S(2)}) collective-permute-start(bf16[1,256,512]{2,1,0:T(8,128)(2,1)S(1)} %select_bitcast_fusion), channel_id=1, source_target_pairs={{0,8},{8,0},{16,24},{24,16},{1,9},{9,1},{17,25},{25,17},{2,10},{10... | collective-permute-start | bytes 786440 | tf_op jit(solution)/shard_map/ppermute | solution.py:31
  5.9 2.7 %collective-permute-start.3 = (bf16[1,128,512]{2,1,0:T(8,128)(2,1)S(1)}, bf16[1,128,512]{2,1,0:T(8,128)(2,1)S(1)}, u32[]{:S(2)}, u32[]{:S(2)}) collective-permute-start(bf16[1,128,512]{2,1,0:T(8,128)(2,1)S(1)} %select_bitcast_fusion.1), channel_id=1, source_target_pairs={{0,16},{8,24},{16,0},{24,8},{1,17},{9,25},{17,1},{25,9},{2,18},{10... | collective-permute-start | bytes 393224 | tf_op jit(solution)/shard_map/ppermute | solution.py:31
  8.5 4.7 %collective-permute-done.3.refs_3_ = bf16[1,128,512]{2,1,0:T(8,128)(2,1)S(1)} collective-permute-done((bf16[1,128,512]{2,1,0:T(8,128)(2,1)S(1)}, bf16[1,128,512]{2,1,0:T(8,128)(2,1)S(1)}, u32[]{:S(2)}, u32[]{:S(2)}) %collective-permute-start.3) | collective-permute-done | bytes 131104 | tf_op jit(solution)/shard_map/ppermute | solution.py:31
  13.2 3.5 %collective-permute-start.7 = (bf16[1,128,512]{2,1,0:T(8,128)(2,1)S(1)}, bf16[1,128,512]{2,1,0:T(8,128)(2,1)S(1)}, u32[]{:S(2)}, u32[]{:S(2)}) collective-permute-start(bf16[1,128,512]{2,1,0:T(8,128)(2,1)S(1)} %collective-permute-done.3.refs_3_), channel_id=1, source_target_pairs={{0,8},{8,0},{16,24},{24,16},{1,9},{9,1},{17,25},{25,17},{2,10},{10... | collective-permute-start | bytes 393224 | tf_op jit(solution)/shard_map/ppermute | solution.py:31
  16.7 2.4 %collective-permute-start.6 = (bf16[1,128,512]{2,1,0:T(8,128)(2,1)S(1)}, bf16[1,128,512]{2,1,0:T(8,128)(2,1)S(1)}, u32[]{:S(2)}, u32[]{:S(2)}) collective-permute-start(bf16[1,128,512]{2,1,0:T(8,128)(2,1)S(1)} %collective-permute-done.3.refs_3_), channel_id=1, source_target_pairs={{0,6},{2,4},{4,2},{6,0},{1,7},{3,5},{5,3},{7,1},{8,14},{10,12},{12... | collective-permute-start | bytes 393224 | tf_op jit(solution)/shard_map/ppermute | solution.py:31
  20.3 1.6 collective-permute-start.2
  23.8 1.8 %collective-permute-start.9 = (bf16[1,128,512]{2,1,0:T(8,128)(2,1)S(1)}, bf16[1,128,512]{2,1,0:T(8,128)(2,1)S(1)}, u32[]{:S(2)}, u32[]{:S(2)}) collective-permute-start(bf16[1,128,512]{2,1,0:T(8,128)(2,1)S(1)} %collective-permute-done.7.refs_7_), channel_id=1, source_target_pairs={{0,4},{2,6},{4,0},{6,2},{1,5},{3,7},{5,1},{7,3},{8,12},{10,14},{12... | collective-permute-start | bytes 393224 | tf_op jit(solution)/shard_map/ppermute | solution.py:31
  25.6 3.3 %collective-permute-done.5.refs_5_ = bf16[1,128,512]{2,1,0:T(8,128)(2,1)S(1)} collective-permute-done((bf16[1,128,512]{2,1,0:T(8,128)(2,1)S(1)}, bf16[1,128,512]{2,1,0:T(8,128)(2,1)S(1)}, u32[]{:S(2)}, u32[]{:S(2)}) %collective-permute-start.5) | collective-permute-done | bytes 131104 | tf_op jit(solution)/shard_map/ppermute | solution.py:31
  40.5 2.7 %tokens.1 = (bf16[2048,512]{1,0:T(8,128)(2,1)S(1)}, bf16[256,512]{1,0:T(8,128)(2,1)S(1)}) custom-call(s32[1]{0:T(128)} %bitcast.z_ref, s32[1]{0:T(128)} %bitcast.1.r_ref, s32[1]{0:T(128)} %bitcast.2.t_ref, bf16[256,2048]{1,0:T(8,128)(2,1)} %x_ref.1, bf16[512,512]{1,0:T(8,128)(2,1)} %own_q_ref.1, bf16[512,512]{1,0:T(8,128)(2,1)} %own_k_ref.1, ...), custom_call_target="tpu_custom_call" | custom-call | tf_op jit(solution)/shard_map/tokens/pallas_call | solution.py:151
  43.3 1.5 collective-permute-done.11.other_ref
  45.7 1.6 terms.1
  47.3 3.5 %all-to-all-start = ((bf16[4,4,32,1280]{3,2,1,0:T(8,128)(2,1)}), bf16[4,4,32,1280]{3,2,1,0:T(8,128)(2,1)S(1)}, u32[]{:S(2)}, u32[]{:S(2)}) async-start(bf16[4,4,32,1280]{3,2,1,0:T(8,128)(2,1)} %terms.1), calls=%async_computation | async-start | bytes 2621440 | tf_op jit(solution)/shard_map/all_to_all | solution.py:35
  50.9 2.1 %dynamic-slice_convert_fusion = (bf16[128,1024]{1,0:T(8,128)(2,1)}, bf16[128,1024]{1,0:T(8,128)(2,1)}) fusion(f32[512,1024]{1,0:T(8,128)} %wq_ref.1, s32[]{:T(128)S(6)} %select_n.41, s32[]{:T(128)S(6)} %select_n.35), kind=kLoop, calls=%fused_computation | loop fusion | bytes 1048584 | tf_op jit(solution)/shard_map/convert_element_type | solution.py:512
  53.1 14.8 %all-to-all-done.in_ref = bf16[4,4,32,1280]{3,2,1,0:T(8,128)(2,1)S(1)} async-done(((bf16[4,4,32,1280]{3,2,1,0:T(8,128)(2,1)}), bf16[4,4,32,1280]{3,2,1,0:T(8,128)(2,1)S(1)}, u32[]{:S(2)}, u32[]{:S(2)}) %all-to-all-start) | async-done | bytes 1310752 | tf_op jit(solution)/shard_map/all_to_all | solution.py:35
  68.7 3.6 %all-to-all-start.1 = ((bf16[4,32,1280]{2,1,0:T(8,128)(2,1)}), bf16[4,32,1280]{2,1,0:T(8,128)(2,1)S(1)}, u32[]{:S(2)}, u32[]{:S(2)}) async-start(bf16[4,32,1280]{2,1,0:T(8,128)(2,1)} %sum_first.1), calls=%async_computation.1 | async-start | bytes 655360 | tf_op jit(solution)/shard_map/all_to_all | solution.py:35
  73.3 1.7 %maximum_bitcast_fusion = bf16[1,128,1280]{2,1,0:T(8,128)(2,1)} fusion(bf16[128,256]{1,0:T(8,128)(2,1)S(1)} %get-tuple-element.41, bf16[128,1024]{1,0:T(8,128)(2,1)} %get-tuple-element.39), kind=kLoop, calls=%fused_computation.2 | loop fusion | flops 655360 | bytes 655360 | tf_op jit(solution)/shard_map/broadcast_in_dim | solution.py:39
  75.0 2.9 %collective-permute-start.16 = (bf16[1,128,1280]{2,1,0:T(8,128)(2,1)}, bf16[1,128,1280]{2,1,0:T(8,128)(2,1)}, u32[]{:S(2)}, u32[]{:S(2)}) collective-permute-start(bf16[1,128,1280]{2,1,0:T(8,128)(2,1)} %maximum_bitcast_fusion), channel_id=1, source_target_pairs={{0,16},{8,24},{16,0},{24,8},{1,17},{9,25},{17,1},{25,9},{2,18},{10... | collective-permute-start | bytes 983048 | tf_op jit(solution)/shard_map/ppermute | solution.py:31
  81.2 9.2 %all-to-all-done.1.got_ref = bf16[4,32,1280]{2,1,0:T(8,128)(2,1)S(1)} async-done(((bf16[4,32,1280]{2,1,0:T(8,128)(2,1)}), bf16[4,32,1280]{2,1,0:T(8,128)(2,1)S(1)}, u32[]{:S(2)}, u32[]{:S(2)}) %all-to-all-start.1) | async-done | bytes 327712 | tf_op jit(solution)/shard_map/all_to_all | solution.py:35
  91.2 3.5 %all-to-all-start.2 = ((bf16[4,32,1280]{2,1,0:T(8,128)(2,1)}), bf16[4,32,1280]{2,1,0:T(8,128)(2,1)S(1)}, u32[]{:S(2)}, u32[]{:S(2)}) async-start(bf16[4,32,1280]{2,1,0:T(8,128)(2,1)} %get-tuple-element.24), calls=%async_computation.2 | async-start | bytes 655360 | tf_op jit(solution)/shard_map/all_to_all | solution.py:35
  95.5 2.9 %collective-permute-start.22 = (bf16[1,128,1280]{2,1,0:T(8,128)(2,1)}, bf16[1,128,1280]{2,1,0:T(8,128)(2,1)}, u32[]{:S(2)}, u32[]{:S(2)}) collective-permute-start(bf16[1,128,1280]{2,1,0:T(8,128)(2,1)} %maximum_bitcast_fusion.1), channel_id=1, source_target_pairs={{0,16},{8,24},{16,0},{24,8},{1,17},{9,25},{17,1},{25,9},{2,18},{10... | collective-permute-start | bytes 983048 | tf_op jit(solution)/shard_map/ppermute | solution.py:31
  98.3 13.1 %all-to-all-done.2.got_ref = bf16[4,32,1280]{2,1,0:T(8,128)(2,1)S(1)} async-done(((bf16[4,32,1280]{2,1,0:T(8,128)(2,1)}), bf16[4,32,1280]{2,1,0:T(8,128)(2,1)S(1)}, u32[]{:S(2)}, u32[]{:S(2)}) %all-to-all-start.2) | async-done | bytes 327712 | tf_op jit(solution)/shard_map/all_to_all | solution.py:35
  112.6 3.5 %all-to-all-start.3 = ((bf16[4,4,32,1280]{3,2,1,0:T(8,128)(2,1)}), bf16[4,4,32,1280]{3,2,1,0:T(8,128)(2,1)S(1)}, u32[]{:S(2)}, u32[]{:S(2)}) async-start(bf16[4,4,32,1280]{3,2,1,0:T(8,128)(2,1)} %plane.1), calls=%async_computation.3 | async-start | bytes 2621440 | tf_op jit(solution)/shard_map/all_to_all | solution.py:35
  116.3 2.0 %collective-permute-start.18 = (bf16[1,128,1280]{2,1,0:T(8,128)(2,1)}, bf16[1,128,1280]{2,1,0:T(8,128)(2,1)}, u32[]{:S(2)}, u32[]{:S(2)}) collective-permute-start(bf16[1,128,1280]{2,1,0:T(8,128)(2,1)} %collective-permute-done.16.refs_2_), channel_id=1, source_target_pairs={{0,8},{8,0},{16,24},{24,16},{1,9},{9,1},{17,25},{25,17},{2,10},{10... | collective-permute-start | bytes 983048 | tf_op jit(solution)/shard_map/ppermute | solution.py:31
  118.3 1.9 %collective-permute-start.17 = (bf16[1,128,1280]{2,1,0:T(8,128)(2,1)}, bf16[1,128,1280]{2,1,0:T(8,128)(2,1)S(1)}, u32[]{:S(2)}, u32[]{:S(2)}) collective-permute-start(bf16[1,128,1280]{2,1,0:T(8,128)(2,1)} %collective-permute-done.16.refs_2_), channel_id=1, source_target_pairs={{0,2},{2,0},{4,6},{6,4},{1,3},{3,1},{5,7},{7,5},{8,10},{10,8},{12,... | collective-permute-start | bytes 983048 | tf_op jit(solution)/shard_map/ppermute | solution.py:31
  120.3 6.9 %collective-permute-done.20.refs_6_ = bf16[1,128,1280]{2,1,0:T(8,128)(2,1)} collective-permute-done((bf16[1,128,1280]{2,1,0:T(8,128)(2,1)}, bf16[1,128,1280]{2,1,0:T(8,128)(2,1)}, u32[]{:S(2)}, u32[]{:S(2)}) %collective-permute-start.20) | collective-permute-done | bytes 327712 | tf_op jit(solution)/shard_map/ppermute | solution.py:31
  127.1 1.9 %collective-permute-start.23 = (bf16[1,128,1280]{2,1,0:T(8,128)(2,1)}, bf16[1,128,1280]{2,1,0:T(8,128)(2,1)S(1)}, u32[]{:S(2)}, u32[]{:S(2)}) collective-permute-start(bf16[1,128,1280]{2,1,0:T(8,128)(2,1)} %collective-permute-done.22.refs_8_), channel_id=1, source_target_pairs={{0,4},{2,6},{4,0},{6,2},{1,5},{3,7},{5,1},{7,3},{8,12},{10,14},{12... | collective-permute-start | bytes 983048 | tf_op jit(solution)/shard_map/ppermute | solution.py:31
  129.1 5.1 %collective-permute-done.18.refs_4_ = bf16[1,128,1280]{2,1,0:T(8,128)(2,1)} collective-permute-done((bf16[1,128,1280]{2,1,0:T(8,128)(2,1)}, bf16[1,128,1280]{2,1,0:T(8,128)(2,1)}, u32[]{:S(2)}, u32[]{:S(2)}) %collective-permute-start.18) | collective-permute-done | bytes 327712 | tf_op jit(solution)/shard_map/ppermute | solution.py:31
  134.2 1.9 %collective-permute-start.15 = (bf16[1,128,1280]{2,1,0:T(8,128)(2,1)}, bf16[1,128,1280]{2,1,0:T(8,128)(2,1)S(1)}, u32[]{:S(2)}, u32[]{:S(2)}) collective-permute-start(bf16[1,128,1280]{2,1,0:T(8,128)(2,1)} %collective-permute-done.14.refs_0_), channel_id=1, source_target_pairs={{0,2},{2,0},{4,6},{6,4},{1,3},{3,1},{5,7},{7,5},{8,10},{10,8},{12,... | collective-permute-start | bytes 983048 | tf_op jit(solution)/shard_map/ppermute | solution.py:31
  136.1 4.9 %collective-permute-done.17.refs_3_ = bf16[1,128,1280]{2,1,0:T(8,128)(2,1)S(1)} collective-permute-done((bf16[1,128,1280]{2,1,0:T(8,128)(2,1)}, bf16[1,128,1280]{2,1,0:T(8,128)(2,1)S(1)}, u32[]{:S(2)}, u32[]{:S(2)}) %collective-permute-start.17) | collective-permute-done | bytes 327712 | tf_op jit(solution)/shard_map/ppermute | solution.py:31
  143.8 4.2 %collective-permute-done.15.refs_1_ = bf16[1,128,1280]{2,1,0:T(8,128)(2,1)S(1)} collective-permute-done((bf16[1,128,1280]{2,1,0:T(8,128)(2,1)}, bf16[1,128,1280]{2,1,0:T(8,128)(2,1)S(1)}, u32[]{:S(2)}, u32[]{:S(2)}) %collective-permute-start.15) | collective-permute-done | bytes 327712 | tf_op jit(solution)/shard_map/ppermute | solution.py:31
  152.9 1.6 directions.1
  155.8 7.1 %finish.1 = (f32[512,1024]{1,0:T(8,128)}, f32[512,256]{1,0:T(8,128)}, f32[512,1024]{1,0:T(8,128)}, f32[512,256]{1,0:T(8,128)}, bf16[2048,1024]{1,0:T(8,128)(2,1)}, /*index=5*/bf16[2048,256]{1,0:T(8,128)(2,1)}) custom-call(s32[1]{0:T(128)} %bitcast.z_ref, s32[1]{0:T(128)} %bitcast.1.r_ref, s32[1]{0:T(128)} %bitcast.2.t_ref, ...), custom_call_target="tpu_custom_call" | custom-call | tf_op jit(solution)/shard_map/finish/pallas_call | solution.py:465
  (85 shorter events, 35.0 us)
Async XLA Ops:
  1.8 18.5 %collective-permute-start = (bf16[1,256,512]{2,1,0:T(8,128)(2,1)S(1)}, bf16[1,256,512]{2,1,0:T(8,128)(2,1)S(1)}, u32[]{:S(2)}, u32[]{:S(2)}) collective-permute-start(bf16[1,256,512]{2,1,0:T(8,128)(2,1)S(1)} %select_bitcast_fusion), channel_id=1, source_target_pairs={{0,8},{8,0},{16,24},{24,16},{1,9},{9,1},{17,25},{25,17},{2,10},{10... | collective-permute-start | bytes 786440 | tf_op jit(solution)/shard_map/ppermute | solution.py:31
  5.9 38.9 %copy-start.1 = (bf16[256,1024]{1,0:T(8,128)(2,1)S(1)}, bf16[256,1024]{1,0:T(8,128)(2,1)}, u32[]{:S(2)}) copy-start(bf16[256,1024]{1,0:T(8,128)(2,1)} %cq_ref.1) | copy-start | bytes 1572868
  5.9 7.4 %collective-permute-start.3 = (bf16[1,128,512]{2,1,0:T(8,128)(2,1)S(1)}, bf16[1,128,512]{2,1,0:T(8,128)(2,1)S(1)}, u32[]{:S(2)}, u32[]{:S(2)}) collective-permute-start(bf16[1,128,512]{2,1,0:T(8,128)(2,1)S(1)} %select_bitcast_fusion.1), channel_id=1, source_target_pairs={{0,16},{8,24},{16,0},{24,8},{1,17},{9,25},{17,1},{25,9},{2,18},{10... | collective-permute-start | bytes 393224 | tf_op jit(solution)/shard_map/ppermute | solution.py:31
  13.2 8.6 %collective-permute-start.7 = (bf16[1,128,512]{2,1,0:T(8,128)(2,1)S(1)}, bf16[1,128,512]{2,1,0:T(8,128)(2,1)S(1)}, u32[]{:S(2)}, u32[]{:S(2)}) collective-permute-start(bf16[1,128,512]{2,1,0:T(8,128)(2,1)S(1)} %collective-permute-done.3.refs_3_), channel_id=1, source_target_pairs={{0,8},{8,0},{16,24},{24,16},{1,9},{9,1},{17,25},{25,17},{2,10},{10... | collective-permute-start | bytes 393224 | tf_op jit(solution)/shard_map/ppermute | solution.py:31
  16.7 7.1 %collective-permute-start.6 = (bf16[1,128,512]{2,1,0:T(8,128)(2,1)S(1)}, bf16[1,128,512]{2,1,0:T(8,128)(2,1)S(1)}, u32[]{:S(2)}, u32[]{:S(2)}) collective-permute-start(bf16[1,128,512]{2,1,0:T(8,128)(2,1)S(1)} %collective-permute-done.3.refs_3_), channel_id=1, source_target_pairs={{0,6},{2,4},{4,2},{6,0},{1,7},{3,5},{5,3},{7,1},{8,14},{10,12},{12... | collective-permute-start | bytes 393224 | tf_op jit(solution)/shard_map/ppermute | solution.py:31
  19.2 9.7 %collective-permute-start.5 = (bf16[1,128,512]{2,1,0:T(8,128)(2,1)S(1)}, bf16[1,128,512]{2,1,0:T(8,128)(2,1)S(1)}, u32[]{:S(2)}, u32[]{:S(2)}) collective-permute-start(bf16[1,128,512]{2,1,0:T(8,128)(2,1)S(1)} %collective-permute-done.3.refs_3_), channel_id=1, source_target_pairs={{0,4},{2,6},{4,0},{6,2},{1,5},{3,7},{5,1},{7,3},{8,12},{10,14},{12... | collective-permute-start | bytes 393224 | tf_op jit(solution)/shard_map/ppermute | solution.py:31
  19.7 10.3 %collective-permute-start.4 = (bf16[1,128,512]{2,1,0:T(8,128)(2,1)S(1)}, bf16[1,128,512]{2,1,0:T(8,128)(2,1)S(1)}, u32[]{:S(2)}, u32[]{:S(2)}) collective-permute-start(bf16[1,128,512]{2,1,0:T(8,128)(2,1)S(1)} %collective-permute-done.3.refs_3_), channel_id=1, source_target_pairs={{0,2},{2,0},{4,6},{6,4},{1,3},{3,1},{5,7},{7,5},{8,10},{10,8},{12,... | collective-permute-start | bytes 393224 | tf_op jit(solution)/shard_map/ppermute | solution.py:31
  20.3 14.3 %collective-permute-start.2 = (bf16[1,128,512]{2,1,0:T(8,128)(2,1)S(1)}, bf16[1,128,512]{2,1,0:T(8,128)(2,1)S(1)}, u32[]{:S(2)}, u32[]{:S(2)}) collective-permute-start(bf16[1,128,512]{2,1,0:T(8,128)(2,1)S(1)} %get-tuple-element.44), channel_id=1, source_target_pairs={{0,4},{2,6},{4,0},{6,2},{1,5},{3,7},{5,1},{7,3},{8,12},{10,14},{12... | collective-permute-start | bytes 393224 | tf_op jit(solution)/shard_map/ppermute | solution.py:31
  21.8 9.1 %collective-permute-start.10 = (bf16[1,128,512]{2,1,0:T(8,128)(2,1)S(1)}, bf16[1,128,512]{2,1,0:T(8,128)(2,1)S(1)}, u32[]{:S(2)}, u32[]{:S(2)}) collective-permute-start(bf16[1,128,512]{2,1,0:T(8,128)(2,1)S(1)} %collective-permute-done.7.refs_7_), channel_id=1, source_target_pairs={{0,6},{2,4},{4,2},{6,0},{1,7},{3,5},{5,3},{7,1},{8,14},{10,12},{12... | collective-permute-start | bytes 393224 | tf_op jit(solution)/shard_map/ppermute | solution.py:31
  23.8 9.1 %collective-permute-start.9 = (bf16[1,128,512]{2,1,0:T(8,128)(2,1)S(1)}, bf16[1,128,512]{2,1,0:T(8,128)(2,1)S(1)}, u32[]{:S(2)}, u32[]{:S(2)}) collective-permute-start(bf16[1,128,512]{2,1,0:T(8,128)(2,1)S(1)} %collective-permute-done.7.refs_7_), channel_id=1, source_target_pairs={{0,4},{2,6},{4,0},{6,2},{1,5},{3,7},{5,1},{7,3},{8,12},{10,14},{12... | collective-permute-start | bytes 393224 | tf_op jit(solution)/shard_map/ppermute | solution.py:31
  28.9 5.0 %collective-permute-start.8 = (bf16[1,128,512]{2,1,0:T(8,128)(2,1)S(1)}, bf16[1,128,512]{2,1,0:T(8,128)(2,1)S(1)}, u32[]{:S(2)}, u32[]{:S(2)}) collective-permute-start(bf16[1,128,512]{2,1,0:T(8,128)(2,1)S(1)} %collective-permute-done.7.refs_7_), channel_id=1, source_target_pairs={{0,2},{2,0},{4,6},{6,4},{1,3},{3,1},{5,7},{7,5},{8,10},{10,8},{12,... | collective-permute-start | bytes 393224 | tf_op jit(solution)/shard_map/ppermute | solution.py:31
  30.0 5.3 %collective-permute-start.1 = (bf16[1,128,512]{2,1,0:T(8,128)(2,1)S(1)}, bf16[1,128,512]{2,1,0:T(8,128)(2,1)S(1)}, u32[]{:S(2)}, u32[]{:S(2)}) collective-permute-start(bf16[1,128,512]{2,1,0:T(8,128)(2,1)S(1)} %get-tuple-element.45), channel_id=1, source_target_pairs={{0,2},{2,0},{4,6},{6,4},{1,3},{3,1},{5,7},{7,5},{8,10},{10,8},{12,... | collective-permute-start | bytes 393224 | tf_op jit(solution)/shard_map/ppermute | solution.py:31
  43.2 1.6 collective-permute-start.11
  47.3 20.5 %all-to-all-start = ((bf16[4,4,32,1280]{3,2,1,0:T(8,128)(2,1)}), bf16[4,4,32,1280]{3,2,1,0:T(8,128)(2,1)S(1)}, u32[]{:S(2)}, u32[]{:S(2)}) async-start(bf16[4,4,32,1280]{3,2,1,0:T(8,128)(2,1)} %terms.1), calls=%async_computation | async-start | bytes 2621440 | tf_op jit(solution)/shard_map/all_to_all | solution.py:35
  52.9 102.9 %collective-permute-start.13 = (bf16[2048,512]{1,0:T(8,128)(2,1)S(1)}, bf16[2048,512]{1,0:T(8,128)(2,1)}, u32[]{:S(2)}, u32[]{:S(2)}) collective-permute-start(bf16[2048,512]{1,0:T(8,128)(2,1)S(1)} %get-tuple-element.29.mine_ref), channel_id=1, source_target_pairs={{0,1},{1,0},{2,3},{3,2},{4,5},{5,4},{6,7},{7,6},{8,9},{9,8},{10,11... | collective-permute-start | bytes 6291464 | tf_op jit(solution)/shard_map/ppermute | solution.py:31
  68.7 21.6 %all-to-all-start.1 = ((bf16[4,32,1280]{2,1,0:T(8,128)(2,1)}), bf16[4,32,1280]{2,1,0:T(8,128)(2,1)S(1)}, u32[]{:S(2)}, u32[]{:S(2)}) async-start(bf16[4,32,1280]{2,1,0:T(8,128)(2,1)} %sum_first.1), calls=%async_computation.1 | async-start | bytes 655360 | tf_op jit(solution)/shard_map/all_to_all | solution.py:35
  75.0 41.2 %collective-permute-start.16 = (bf16[1,128,1280]{2,1,0:T(8,128)(2,1)}, bf16[1,128,1280]{2,1,0:T(8,128)(2,1)}, u32[]{:S(2)}, u32[]{:S(2)}) collective-permute-start(bf16[1,128,1280]{2,1,0:T(8,128)(2,1)} %maximum_bitcast_fusion), channel_id=1, source_target_pairs={{0,16},{8,24},{16,0},{24,8},{1,17},{9,25},{17,1},{25,9},{2,18},{10... | collective-permute-start | bytes 983048 | tf_op jit(solution)/shard_map/ppermute | solution.py:31
  77.9 40.4 %collective-permute-start.14 = (bf16[1,128,1280]{2,1,0:T(8,128)(2,1)}, bf16[1,128,1280]{2,1,0:T(8,128)(2,1)}, u32[]{:S(2)}, u32[]{:S(2)}) collective-permute-start(bf16[1,128,1280]{2,1,0:T(8,128)(2,1)} %maximum_bitcast_fusion), channel_id=1, source_target_pairs={{0,8},{8,0},{16,24},{24,16},{1,9},{9,1},{17,25},{25,17},{2,10},{10... | collective-permute-start | bytes 983048 | tf_op jit(solution)/shard_map/ppermute | solution.py:31
  91.2 20.2 %all-to-all-start.2 = ((bf16[4,32,1280]{2,1,0:T(8,128)(2,1)}), bf16[4,32,1280]{2,1,0:T(8,128)(2,1)S(1)}, u32[]{:S(2)}, u32[]{:S(2)}) async-start(bf16[4,32,1280]{2,1,0:T(8,128)(2,1)} %get-tuple-element.24), calls=%async_computation.2 | async-start | bytes 655360 | tf_op jit(solution)/shard_map/all_to_all | solution.py:35
  95.5 24.7 %collective-permute-start.22 = (bf16[1,128,1280]{2,1,0:T(8,128)(2,1)}, bf16[1,128,1280]{2,1,0:T(8,128)(2,1)}, u32[]{:S(2)}, u32[]{:S(2)}) collective-permute-start(bf16[1,128,1280]{2,1,0:T(8,128)(2,1)} %maximum_bitcast_fusion.1), channel_id=1, source_target_pairs={{0,16},{8,24},{16,0},{24,8},{1,17},{9,25},{17,1},{25,9},{2,18},{10... | collective-permute-start | bytes 983048 | tf_op jit(solution)/shard_map/ppermute | solution.py:31
  112.6 38.1 %all-to-all-start.3 = ((bf16[4,4,32,1280]{3,2,1,0:T(8,128)(2,1)}), bf16[4,4,32,1280]{3,2,1,0:T(8,128)(2,1)S(1)}, u32[]{:S(2)}, u32[]{:S(2)}) async-start(bf16[4,4,32,1280]{3,2,1,0:T(8,128)(2,1)} %plane.1), calls=%async_computation.3 | async-start | bytes 2621440 | tf_op jit(solution)/shard_map/all_to_all | solution.py:35
  116.2 11.0 %collective-permute-start.20 = (bf16[1,128,1280]{2,1,0:T(8,128)(2,1)}, bf16[1,128,1280]{2,1,0:T(8,128)(2,1)}, u32[]{:S(2)}, u32[]{:S(2)}) collective-permute-start(bf16[1,128,1280]{2,1,0:T(8,128)(2,1)} %maximum_bitcast_fusion.1), channel_id=1, source_target_pairs={{0,8},{8,0},{16,24},{24,16},{1,9},{9,1},{17,25},{25,17},{2,10},{10... | collective-permute-start | bytes 983048 | tf_op jit(solution)/shard_map/ppermute | solution.py:31
  116.3 17.9 %collective-permute-start.18 = (bf16[1,128,1280]{2,1,0:T(8,128)(2,1)}, bf16[1,128,1280]{2,1,0:T(8,128)(2,1)}, u32[]{:S(2)}, u32[]{:S(2)}) collective-permute-start(bf16[1,128,1280]{2,1,0:T(8,128)(2,1)} %collective-permute-done.16.refs_2_), channel_id=1, source_target_pairs={{0,8},{8,0},{16,24},{24,16},{1,9},{9,1},{17,25},{25,17},{2,10},{10... | collective-permute-start | bytes 983048 | tf_op jit(solution)/shard_map/ppermute | solution.py:31
  118.3 22.7 %collective-permute-start.17 = (bf16[1,128,1280]{2,1,0:T(8,128)(2,1)}, bf16[1,128,1280]{2,1,0:T(8,128)(2,1)S(1)}, u32[]{:S(2)}, u32[]{:S(2)}) collective-permute-start(bf16[1,128,1280]{2,1,0:T(8,128)(2,1)} %collective-permute-done.16.refs_2_), channel_id=1, source_target_pairs={{0,2},{2,0},{4,6},{6,4},{1,3},{3,1},{5,7},{7,5},{8,10},{10,8},{12,... | collective-permute-start | bytes 983048 | tf_op jit(solution)/shard_map/ppermute | solution.py:31
  120.2 22.2 %collective-permute-start.24 = (bf16[1,128,1280]{2,1,0:T(8,128)(2,1)}, bf16[1,128,1280]{2,1,0:T(8,128)(2,1)S(1)}, u32[]{:S(2)}, u32[]{:S(2)}) collective-permute-start(bf16[1,128,1280]{2,1,0:T(8,128)(2,1)} %collective-permute-done.22.refs_8_), channel_id=1, source_target_pairs={{0,8},{8,0},{16,24},{24,16},{1,9},{9,1},{17,25},{25,17},{2,10},{10... | collective-permute-start | bytes 983048 | tf_op jit(solution)/shard_map/ppermute | solution.py:31
  127.1 22.3 %collective-permute-start.23 = (bf16[1,128,1280]{2,1,0:T(8,128)(2,1)}, bf16[1,128,1280]{2,1,0:T(8,128)(2,1)S(1)}, u32[]{:S(2)}, u32[]{:S(2)}) collective-permute-start(bf16[1,128,1280]{2,1,0:T(8,128)(2,1)} %collective-permute-done.22.refs_8_), channel_id=1, source_target_pairs={{0,4},{2,6},{4,0},{6,2},{1,5},{3,7},{5,1},{7,3},{8,12},{10,14},{12... | collective-permute-start | bytes 983048 | tf_op jit(solution)/shard_map/ppermute | solution.py:31
  134.2 13.8 %collective-permute-start.15 = (bf16[1,128,1280]{2,1,0:T(8,128)(2,1)}, bf16[1,128,1280]{2,1,0:T(8,128)(2,1)S(1)}, u32[]{:S(2)}, u32[]{:S(2)}) collective-permute-start(bf16[1,128,1280]{2,1,0:T(8,128)(2,1)} %collective-permute-done.14.refs_0_), channel_id=1, source_target_pairs={{0,2},{2,0},{4,6},{6,4},{1,3},{3,1},{5,7},{7,5},{8,10},{10,8},{12,... | collective-permute-start | bytes 983048 | tf_op jit(solution)/shard_map/ppermute | solution.py:31
  141.0 13.6 %collective-permute-start.21 = (bf16[1,128,1280]{2,1,0:T(8,128)(2,1)}, bf16[1,128,1280]{2,1,0:T(8,128)(2,1)}, u32[]{:S(2)}, u32[]{:S(2)}) collective-permute-start(bf16[1,128,1280]{2,1,0:T(8,128)(2,1)} %collective-permute-done.20.refs_6_), channel_id=1, source_target_pairs={{0,4},{2,6},{4,0},{6,2},{1,5},{3,7},{5,1},{7,3},{8,12},{10,14},{12... | collective-permute-start | bytes 983048 | tf_op jit(solution)/shard_map/ppermute | solution.py:31
  142.4 13.4 %collective-permute-start.19 = (bf16[1,128,1280]{2,1,0:T(8,128)(2,1)}, bf16[1,128,1280]{2,1,0:T(8,128)(2,1)}, u32[]{:S(2)}, u32[]{:S(2)}) collective-permute-start(bf16[1,128,1280]{2,1,0:T(8,128)(2,1)} %collective-permute-done.18.refs_4_), channel_id=1, source_target_pairs={{0,2},{2,0},{4,6},{6,4},{1,3},{3,1},{5,7},{7,5},{8,10},{10,8},{12,... | collective-permute-start | bytes 983048 | tf_op jit(solution)/shard_map/ppermute | solution.py:31
  148.0 6.5 %collective-permute-start.26 = (bf16[1,64,1280]{2,1,0:T(8,128)(2,1)}, bf16[1,64,1280]{2,1,0:T(8,128)(2,1)}, u32[]{:S(2)}, u32[]{:S(2)}) collective-permute-start(bf16[1,64,1280]{2,1,0:T(8,128)(2,1)} %get-tuple-element.42), channel_id=1, source_target_pairs={{0,4},{2,6},{4,0},{6,2},{1,5},{3,7},{5,1},{7,3},{8,12},{10,14},{12... | collective-permute-start | bytes 491528 | tf_op jit(solution)/shard_map/ppermute | solution.py:31
  150.2 5.6 %collective-permute-start.25 = (bf16[1,64,1280]{2,1,0:T(8,128)(2,1)}, bf16[1,64,1280]{2,1,0:T(8,128)(2,1)}, u32[]{:S(2)}, u32[]{:S(2)}) collective-permute-start(bf16[1,64,1280]{2,1,0:T(8,128)(2,1)} %get-tuple-element.43), channel_id=1, source_target_pairs={{0,2},{2,0},{4,6},{6,4},{1,3},{3,1},{5,7},{7,5},{8,10},{10,8},{12,... | collective-permute-start | bytes 491528 | tf_op jit(solution)/shard_map/ppermute | solution.py:31
  154.5 1.3 collective-permute-start.12
  (18 other events, 47.5 us)
